TPU v7x, 32 devices: a whole 2x2x4 slice. The times are simulated.
32 devices in a mesh: sp: 16 (over z, y, core), tp: 2 (over x).
Axes of the slice: x: 2, y: 2, z: 4, core: 2. Of those that a mesh axis runs over, the one named last changes fastest.
Arguments:
- stream: bfloat16 [2048, 2048], P('sp', 'tp'), may hold values from -52 to 52
- norm_gain: float32 [2, 2048], replicated, may hold values from 0.1 to 1.9
- value_weight: bfloat16 [4096, 1024], P('sp', 'tp'), may hold values from -0.125 to 0.125
- gate_weight: bfloat16 [4096, 1024], P('sp', 'tp'), may hold values from -0.125 to 0.125
- conv_taps: float32 [2, 31, 1024], replicated, may hold values from -3 to 3
- ln_gain: float32 [2, 1024], replicated, may hold values from 0.1 to 1.9
- ln_bias: float32 [2, 1024], replicated, may hold values from -3 to 3
- out_weight: bfloat16 [1024, 4096], P('tp', 'sp'), may hold values from -0.1875 to 0.1875
- final_gain: float32 [2048], replicated, may hold values from 0.1 to 1.9
Outputs:
- result: bfloat16 [2048, 2048], P('sp', 'tp')
All inputs are finite; a program needn't handle non-finite values.
Results may differ from a plain program's by a relative error of at most 0.014.
Values may be sent and summed in bfloat16 or wider, within the bound.
A program may use at most 64 MiB of HBM per device.

v0:
```python
import functools

import jax
import jax.numpy as jnp
from jax import lax
from jax.experimental import pallas as pl
from jax.experimental.pallas import tpu as pltpu
from jax.sharding import PartitionSpec as P

D = 2048
C = 1024
KW = 31
LAYERS = 2


EPS = 1e-06


def from_behind(value, axis, steps):
    count = lax.axis_size(axis)
    first, last = (max(0, -steps), min(count, count - steps))
    return lax.ppermute(value, axis, [(source, source + steps) for source in range(first, last)])


def valid_conv(extended, tap_table):
    length = extended.shape[0] - (KW - 1)
    running = tap_table[0] * extended[0:length]
    for tap_index in range(1, KW):
        running = running + tap_table[tap_index] * extended[tap_index : tap_index + length]
    return running


def local(
    stream,
    norm_gain,
    value_weight,
    gate_weight,
    conv_taps,
    ln_gain,
    ln_bias,
    out_weight,
    final_gain,
):
    tokens_here = stream.shape[0]
    columns = stream.shape[1]
    channels = value_weight.shape[1]
    rim_rows = KW - 1
    tp_index = lax.axis_index("tp")
    my_taps = lax.dynamic_slice_in_dim(conv_taps, tp_index * channels, channels, 2)
    my_ln_gain = lax.dynamic_slice_in_dim(ln_gain, tp_index * channels, channels, 1)
    my_ln_bias = lax.dynamic_slice_in_dim(ln_bias, tp_index * channels, channels, 1)
    my_final = lax.dynamic_slice_in_dim(final_gain, tp_index * columns, columns, 0)
    value_all, gate_all, out_all = (
        lax.all_gather(value_weight, "sp", axis=0, tiled=True),
        lax.all_gather(gate_weight, "sp", axis=0, tiled=True),
        lax.all_gather(out_weight, "sp", axis=1, tiled=True),
    )
    value_all = value_all.reshape(D, LAYERS, channels)
    gate_all = gate_all.reshape(D, LAYERS, channels)
    out_all = out_all.reshape(channels, D, LAYERS)
    earlier = from_behind(stream[-LAYERS * rim_rows :], "sp", 1)
    current = jnp.concatenate([earlier, stream], axis=0)
    for layer_index in range(LAYERS):
        prefix = (LAYERS - layer_index) * rim_rows
        gathered = lax.all_gather(current, "tp", axis=1, tiled=True)
        gathered32 = gathered.astype(jnp.float32)
        scale = lax.rsqrt(jnp.sum(gathered32 * gathered32, axis=1, keepdims=True) / D + EPS)
        run_normed = (gathered32 * scale * norm_gain[layer_index]).astype(jnp.bfloat16)
        value_proj = jnp.dot(
            run_normed, value_all[:, layer_index], preferred_element_type=jnp.float32
        )
        gate_proj = jnp.dot(
            run_normed, gate_all[:, layer_index], preferred_element_type=jnp.float32
        )
        glu_out = value_proj * jax.nn.sigmoid(gate_proj)
        positions = (
            lax.axis_index("sp") * tokens_here - prefix + lax.iota(jnp.int32, current.shape[0])
        )
        extended = jnp.where((positions >= 0)[:, None], glu_out, 0.0)
        residual = current[rim_rows:].astype(jnp.float32)
        conv_out = valid_conv(extended, my_taps[layer_index])
        first_sums, square_sums = lax.psum(
            (jnp.sum(conv_out, axis=1), jnp.sum(conv_out * conv_out, axis=1)), "tp"
        )
        row_mean = (first_sums / C)[:, None]
        row_var = (square_sums / C)[:, None] - row_mean * row_mean
        run_active = jax.nn.silu(
            (conv_out - row_mean) * lax.rsqrt(row_var + EPS) * my_ln_gain[layer_index]
            + my_ln_bias[layer_index]
        ).astype(jnp.bfloat16)
        partial_value = jnp.dot(
            run_active, out_all[:, :, layer_index], preferred_element_type=jnp.float32
        )
        summed = lax.psum_scatter(
            partial_value.astype(jnp.bfloat16), "tp", scatter_dimension=1, tiled=True
        ).astype(jnp.float32)
        current = (residual + summed).astype(jnp.bfloat16)
    final32 = current.astype(jnp.float32)
    squares = lax.psum(jnp.sum(final32 * final32, axis=1), "tp")
    return (final32 * lax.rsqrt(squares[:, None] / D + EPS) * my_final).astype(jnp.bfloat16)


MESH = pl.DeviceIdType.MESH
HALO = 32
UP, DOWN, SIDE, CORE = range(4)
ITEMS = 3 * LAYERS
PAIRED = (0, 2, 4)


def fused_kernel(
    n, x_in, ng_in, v_in, g_in, taps_in, lng_in, lnb_in, o_in, fg_in, out_ref,
    x_ref, ng_ref, v_ref, g_ref, taps_ref, lng_ref, lnb_ref, o_ref, fg_ref, isem, vg, ob, xf, xn, nb, ext, cv, act, part, rpart, st, rst,
    ssem, rsem, xsem, hsem, tsem, psem,
):
    loads = [
        pltpu.make_async_copy(source, to, isem.at[i])
        for i, (source, to) in enumerate((
            (v_in, v_ref), (g_in, g_ref), (x_in, x_ref), (o_in, o_ref), (ng_in, ng_ref),
            (taps_in, taps_ref), (lng_in, lng_ref), (lnb_in, lnb_ref), (fg_in, fg_ref)))
    ]
    for load in loads:
        load.start()
    levels = n // 4
    sp = lax.axis_index("sp")
    tp = lax.axis_index("tp")
    z, y, core = sp // 4, (sp // 2) % 2, sp % 2
    peer = 1 - tp
    rows, cols = x_ref.shape
    depth = v_ref.shape[0] // LAYERS
    ch = v_ref.shape[1]
    width = o_ref.shape[1] // LAYERS
    has_up, has_down = z < levels - 1, z > 0
    even, odd = z % 2 == 0, z % 2 == 1
    target = {UP: sp + 4, DOWN: sp - 4, SIDE: sp + 2 - 4 * y, CORE: sp + 1 - 2 * core}

    def slot(k, src):
        layer, kind = divmod(k, 3)
        return ob.at[layer, src] if kind == 2 else vg.at[layer * 2 + kind, src]

    def copy(k, src, way):
        return pltpu.make_async_remote_copy(
            src_ref=slot(k, src), dst_ref=slot(k, src),
            send_sem=ssem.at[k, way, src], recv_sem=rsem.at[k, src],
            device_id={"sp": target[way], "tp": tp}, device_id_type=MESH)

    def index(zz, yy, cc):
        return (zz * 2 + yy) * 2 + cc

    def own(k, act_on):
        act_on(k, sp, SIDE)
        pl.when(has_up)(lambda: act_on(k, sp, UP))
        pl.when(has_down)(lambda: act_on(k, sp, DOWN))
        act_on(k, sp, CORE)

    def line(k, act_on, wait, steps=None):
        def one(src, way, more, to_side):
            if wait:
                copy(k, src, way).wait_recv()
            if to_side is not None:
                pl.when(to_side)(lambda: act_on(k, src, SIDE))
            else:
                act_on(k, src, SIDE)
            pl.when(more)(lambda: act_on(k, src, way))
            act_on(k, src, CORE)

        paired = k in PAIRED
        for d in steps or range(1, levels):
            near = paired and d == 1
            pl.when(z - d >= 0)(lambda: one(index(z - d, y, core), UP, has_up, even if near else None))
            pl.when(z + d < levels)(lambda: one(index(z + d, y, core), DOWN, has_down, odd if near else None))
            if d == 1:
                first = index(z, 1 - y, core)
                if wait:
                    copy(k, first, SIDE).wait_recv()
                if paired:
                    pl.when(even)(lambda: act_on(k, first, UP))
                    pl.when(odd)(lambda: act_on(k, first, DOWN))
                act_on(k, first, CORE)

    def across(k, act_on, wait, then=None):
        def one(zz):
            src = index(zz, 1 - y, core)
            if wait:
                copy(k, src, SIDE).wait_recv()
            act_on(k, src, CORE)
            if then is not None:
                then(zz, 1 - y)

        for d in range(1, levels):
            pl.when(z - d >= 0)(lambda: one(z - d))
            pl.when(z + d < levels)(lambda: one(z + d))

    def other_core(k):
        for zz in range(levels):
            for yy in range(2):
                copy(k, index(zz, yy, 1 - core), CORE).wait_recv()

    def start(k, src, way):
        copy(k, src, way).start()

    def finish(k, src, way):
        copy(k, src, way).wait_send()

    def to_peer(src, dst, sems):
        return pltpu.make_async_remote_copy(
            src_ref=src, dst_ref=dst, send_sem=sems[0], recv_sem=sems[1],
            device_id={"sp": sp, "tp": peer}, device_id_type=MESH)

    def halo(layer):
        return pltpu.make_async_remote_copy(
            src_ref=ext.at[layer, pl.ds(rows, HALO)], dst_ref=ext.at[layer, pl.ds(0, HALO)],
            send_sem=hsem.at[layer, 0], recv_sem=hsem.at[layer, 1],
            device_id={"sp": sp + 1, "tp": tp}, device_id_type=MESH)

    barrier = pltpu.get_barrier_semaphore()

    def greet(device):
        pl.semaphore_signal(barrier, inc=1, device_id=device, device_id_type=MESH)

    greet({"sp": target[SIDE], "tp": tp})
    greet({"sp": target[CORE], "tp": tp})
    greet({"sp": sp, "tp": peer})
    pl.when(has_up)(lambda: greet({"sp": target[UP], "tp": tp}))
    pl.when(has_down)(lambda: greet({"sp": target[DOWN], "tp": tp}))
    pl.when(sp < n - 1)(lambda: greet({"sp": sp + 1, "tp": tp}))
    pl.when(sp > 0)(lambda: greet({"sp": sp - 1, "tp": tp}))

    lo = lax.broadcasted_iota(jnp.int32, (depth, LAYERS * depth), 0)
    hi = lax.broadcasted_iota(jnp.int32, (depth, LAYERS * depth), 1)
    clo = lax.broadcasted_iota(jnp.int32, (LAYERS * width, width), 1)
    chi = lax.broadcasted_iota(jnp.int32, (LAYERS * width, width), 0)

    def pick_rows(kind, ref):
        for layer in range(LAYERS):
            pick = (hi == LAYERS * lo + layer).astype(jnp.float32).astype(jnp.bfloat16)
            vg[layer * 2 + kind, sp] = jnp.dot(
                pick, ref[...], preferred_element_type=jnp.float32).astype(jnp.bfloat16)

    def pick_columns():
        for layer in range(LAYERS):
            pick = (chi == LAYERS * clo + layer).astype(jnp.float32).astype(jnp.bfloat16)
            ob[layer, sp] = jnp.dot(
                o_ref[...], pick, preferred_element_type=jnp.float32).astype(jnp.bfloat16)

    loads[0].wait()
    pick_rows(0, v_ref)

    @pl.when(sp == 0)
    def _():
        for layer in range(LAYERS):
            ext[layer, 0:HALO] = jnp.zeros((HALO, ch), jnp.float32)

    ends = [has_up, has_down, sp < n - 1, sp > 0]
    pl.semaphore_wait(barrier, 3 + sum(end.astype(jnp.int32) for end in ends))

    own(0, start)
    loads[2].wait()
    x_copy = to_peer(x_ref, xf.at[tp], (xsem.at[0], xsem.at[1]))
    x_copy.start()
    loads[1].wait()
    pick_rows(1, g_ref)
    own(1, start)
    xf[tp] = x_ref[...]
    loads[3].wait()
    pick_columns()
    for load in loads[4:]:
        load.wait()

    def normalise(source, layer):
        total = jnp.zeros((rows, 1), jnp.float32)
        for half in range(2):
            value = source[half].astype(jnp.float32)
            total = total + jnp.sum(value * value, axis=1, keepdims=True)
        scale = lax.rsqrt(total / D + EPS)
        for half in range(2):
            value = source[half].astype(jnp.float32)
            gain = ng_ref[layer : layer + 1, half * cols : (half + 1) * cols]
            nb[:, half * cols : (half + 1) * cols] = (value * scale * gain).astype(jnp.bfloat16)

    def glu(layer):
        value, gate = (
            jnp.dot(nb[...], vg[layer * 2 + kind].reshape(n * depth, ch),
                    preferred_element_type=jnp.float32) for kind in range(2))
        ext[layer, HALO:] = value * jax.nn.sigmoid(gate)
        pl.when(sp < n - 1)(lambda: halo(layer).start())

    def stat_copy(i):
        return to_peer(st.at[i], rst.at[i], (tsem.at[i, 0], tsem.at[i, 1]))

    def send_stats(i, first, second):
        lane = lax.broadcasted_iota(jnp.int32, (rows, 128), 1)
        turned = jnp.where(lane < 64, first, second).T
        st[i, 0:8] = turned[0:8]
        st[i, 8:16] = turned[64:72]
        stat_copy(i).start()

    def take_stats(i):
        stat_copy(i).wait_recv()
        both = st[i] + rst[i]
        turned = jnp.concatenate([both] * (128 // 16), axis=0).T
        return turned[:, 0:1], turned[:, 8:9]

    def conv(layer):
        tap_cols = pl.ds(pl.multiple_of(tp * ch, 128), ch)

        def chunk(r0):
            running = jnp.zeros((HALO, ch), jnp.float32)
            for k in range(KW):
                at = r0 + k + HALO - (KW - 1)
                running = running + taps_ref[k, layer : layer + 1, tap_cols] * ext[layer, at : at + HALO]
            cv[r0 : r0 + HALO] = running

        for r0 in range(HALO, rows, HALO):
            chunk(r0)
        pl.when(sp > 0)(lambda: halo(layer).wait_recv())
        chunk(0)
        value = cv[...]
        send_stats(layer, jnp.sum(value, axis=1, keepdims=True),
                   jnp.sum(value * value, axis=1, keepdims=True))

    def activate(layer):
        first, second = take_stats(layer)
        mean = first / C
        var = second / C - mean * mean
        here = pl.ds(pl.multiple_of(tp * ch, 128), ch)
        v = (cv[...] - mean) * lax.rsqrt(var + EPS) * lng_ref[layer : layer + 1, here]
        v = v + lnb_ref[layer : layer + 1, here]
        act[...] = (v / (1.0 + jnp.exp(-v))).astype(jnp.bfloat16)

    pairs = n // 2
    half_pairs = pairs // 2

    def part_copy(layer, p):
        return to_peer(part.at[layer, p], rpart.at[layer, p], (psem.at[layer, 0, p], psem.at[layer, 1, p]))

    def project(layer, p):
        weights = jnp.concatenate([ob[layer, 2 * p], ob[layer, 2 * p + 1]], axis=1)
        part[layer, p] = jnp.dot(
            act[...], weights, preferred_element_type=jnp.float32).astype(jnp.bfloat16)

    def add_parts(layer, p):
        return part[layer, p].astype(jnp.float32) + rpart[layer, p].astype(jnp.float32)

    def project_last(zz, yy):
        p = zz * 2 + yy
        copy(ITEMS - 1, index(zz, yy, 1 - core), CORE).wait_recv()
        project(LAYERS - 1, p)
        pl.when(p // half_pairs == peer)(lambda: part_copy(LAYERS - 1, p).start())

    own(2, start)
    line(0, start, True)
    x_copy.wait_recv()
    normalise(xf, 0)
    own(3, start)
    line(1, start, True)
    across(0, start, True)
    own(4, start)
    near, far = range(1, levels - 1), range(levels - 1, levels)
    line(2, start, True, near)
    across(1, start, True)
    own(5, start)
    other_core(0)
    other_core(1)
    glu(0)
    line(2, start, True, far)
    line(3, start, True, near)
    conv(0)
    line(3, start, True, far)
    across(2, start, True)
    activate(0)
    other_core(2)
    for p in range(pairs):
        project(0, p)
        part_copy(0, p).start()
        if p == half_pairs:
            line(4, start, True, near)
    line(4, start, True, far)
    across(3, start, True)
    line(5, start, True)
    for p in range(pairs):
        part_copy(0, p).wait_recv()
        half, at = p // half_pairs, (p % half_pairs) * 2 * width
        here = xf[half, :, at : at + 2 * width].astype(jnp.float32)
        xn[half, :, at : at + 2 * width] = (here + add_parts(0, p)).astype(jnp.bfloat16)
    normalise(xn, 1)
    across(4, start, True)
    other_core(3)
    other_core(4)
    glu(1)
    conv(1)
    activate(1)
    project_last(z, y)
    for d in range(1, levels):
        pl.when(z - d >= 0)(lambda: project_last(z - d, y))
        pl.when(z + d < levels)(lambda: project_last(z + d, y))
    project_last(z, 1 - y)
    across(5, start, True, project_last)
    squares = jnp.zeros((rows, 1), jnp.float32)
    for q in range(half_pairs):
        p = tp * half_pairs + q
        part_copy(1, p).wait_recv()
        at = q * 2 * width
        here = xn[tp, :, at : at + 2 * width].astype(jnp.float32)
        fresh = (here + add_parts(1, p)).astype(jnp.bfloat16)
        out_ref[:, at : at + 2 * width] = fresh
        fresh = fresh.astype(jnp.float32)
        squares = squares + jnp.sum(fresh * fresh, axis=1, keepdims=True)
    send_stats(LAYERS, squares, squares)
    total, _ = take_stats(LAYERS)
    gain = fg_ref[0:1, pl.ds(pl.multiple_of(tp * cols, 128), cols)]
    out_ref[...] = (
        out_ref[...].astype(jnp.float32) * lax.rsqrt(total / D + EPS) * gain).astype(jnp.bfloat16)

    for k in range(ITEMS):
        own(k, finish)
        line(k, finish, False)
        across(k, finish, False)
    x_copy.wait_send()
    for layer in range(LAYERS):
        pl.when(sp < n - 1)(lambda: halo(layer).wait_send())
    for i in range(LAYERS + 1):
        stat_copy(i).wait_send()
    for p in range(pairs):
        part_copy(0, p).wait_send()
    for q in range(half_pairs):
        part_copy(1, peer * half_pairs + q).wait_send()


def fused(n, stream, norm_gain, value_weight, gate_weight, conv_taps, ln_gain, ln_bias, out_weight, final_gain):
    rows, cols = stream.shape
    depth, ch = value_weight.shape[0] // LAYERS, value_weight.shape[1]
    width = out_weight.shape[1] // LAYERS
    bf16, f32 = jnp.bfloat16, jnp.float32
    dma = pltpu.SemaphoreType.DMA
    arrays = (stream, norm_gain, value_weight, gate_weight, conv_taps.transpose(1, 0, 2),
              ln_gain, ln_bias, out_weight, final_gain.reshape(1, -1))
    return pl.pallas_call(
        functools.partial(fused_kernel, n),
        out_shape=jax.ShapeDtypeStruct((rows, cols), bf16),
        in_specs=[pl.BlockSpec(memory_space=pl.ANY)] * 9,
        out_specs=pl.BlockSpec(memory_space=pltpu.VMEM),
        scratch_shapes=[pltpu.VMEM(array.shape, array.dtype) for array in arrays] + [
            dma((len(arrays),)),
            pltpu.VMEM((2 * LAYERS, n, depth, ch), bf16),
            pltpu.VMEM((LAYERS, n, ch, width), bf16),
            pltpu.VMEM((2, rows, cols), bf16),
            pltpu.VMEM((2, rows, cols), bf16),
            pltpu.VMEM((rows, 2 * cols), bf16),
            pltpu.VMEM((LAYERS, HALO + rows, ch), f32),
            pltpu.VMEM((rows, ch), f32),
            pltpu.VMEM((rows, ch), bf16),
            pltpu.VMEM((LAYERS, n // 2, rows, 2 * width), bf16),
            pltpu.VMEM((LAYERS, n // 2, rows, 2 * width), bf16),
            pltpu.VMEM((LAYERS + 1, 16, rows), f32),
            pltpu.VMEM((LAYERS + 1, 16, rows), f32),
            dma((ITEMS, 4, n)),
            dma((ITEMS, n)),
            dma((2,)),
            dma((LAYERS, 2)),
            dma((LAYERS + 1, 2)),
            dma((LAYERS, 2, n // 2)),
        ],
        compiler_params=pltpu.CompilerParams(collective_id=0, has_side_effects=True),
    )(*arrays)


def solution(mesh):
    placed = (P("sp", "tp"), P(), P("sp", "tp"), P("sp", "tp"), P(), P(), P(), P("tp", "sp"), P())
    n, n_tp = mesh.shape["sp"], mesh.shape["tp"]

    def step(*args):
        stream, out_weight = args[0], args[7]
        fits = n_tp == 2 and n % 8 == 0 and stream.shape[0] == 128 and out_weight.shape[1] == 128 * LAYERS
        return fused(n, *args) if fits else local(*args)

    return jax.shard_map(step, mesh=mesh, in_specs=placed, out_specs=P("sp", "tp"), check_vma=False)
```

profile of v0, /device:TPU:4, one launch (start us, length us, event | category | flops | bytes accessed | tf_op | source)
XLA Modules:
  0.0 92.8 jit_solution(14717096316596971419)
XLA Ops:
  0.0 91.2 %shard_map.91 = bf16[128,1024]{1,0:T(8,128)(2,1)} custom-call(bf16[128,1024]{1,0:T(8,128)(2,1)} %x_in.1, f32[2,2048]{1,0:T(2,128)} %ng_in.1, bf16[256,512]{1,0:T(8,128)(2,1)} %v_in.1, bf16[256,512]{1,0:T(8,128)(2,1)} %g_in.1, f32[31,2,1024]{2,1,0:T(2,128)} %bitcast.2, f32[2,1024]{1,0:T(2,128)} %lng_in.1, f32[2,1024]{1,0:T(2,128)} %lnb_in.1, ...), custom_call_target="tpu_custom_call" | custom-call | tf_op jit(solution)/shard_map/pallas_call | solution.py:437
  91.2 1.7 %copy.11 = bf16[128,1024]{1,0:T(8,128)(2,1)} copy(bf16[128,1024]{1,0:T(8,128)(2,1)} %shard_map.91) | data formatting | bytes 524288
where the time goes:
time: 93 us; the launch traced here: 92.8 us
  Pallas kernels  91.2 us (98%)
  local copies, waits for them, and re-layouts  1.67 us (2%)
    pallas_call x1, Pallas kernels, fused(): pl.pallas_call(functools.partial(fused_kernel, n), out_shape=jax.ShapeDty...  91.2 us

commit v1 on v0

v1 whole, which is shorter than its diff:
```python
import functools

import jax
import jax.numpy as jnp
from jax import lax
from jax.experimental import pallas as pl
from jax.experimental.pallas import tpu as pltpu
from jax.sharding import PartitionSpec as P

D = 2048
C = 1024
KW = 31
LAYERS = 2


EPS = 1e-06


def from_behind(value, axis, steps):
    count = lax.axis_size(axis)
    first, last = (max(0, -steps), min(count, count - steps))
    return lax.ppermute(value, axis, [(source, source + steps) for source in range(first, last)])


def valid_conv(extended, tap_table):
    length = extended.shape[0] - (KW - 1)
    running = tap_table[0] * extended[0:length]
    for tap_index in range(1, KW):
        running = running + tap_table[tap_index] * extended[tap_index : tap_index + length]
    return running


def local(
    stream,
    norm_gain,
    value_weight,
    gate_weight,
    conv_taps,
    ln_gain,
    ln_bias,
    out_weight,
    final_gain,
):
    tokens_here = stream.shape[0]
    columns = stream.shape[1]
    channels = value_weight.shape[1]
    rim_rows = KW - 1
    tp_index = lax.axis_index("tp")
    my_taps = lax.dynamic_slice_in_dim(conv_taps, tp_index * channels, channels, 2)
    my_ln_gain = lax.dynamic_slice_in_dim(ln_gain, tp_index * channels, channels, 1)
    my_ln_bias = lax.dynamic_slice_in_dim(ln_bias, tp_index * channels, channels, 1)
    my_final = lax.dynamic_slice_in_dim(final_gain, tp_index * columns, columns, 0)
    value_all, gate_all, out_all = (
        lax.all_gather(value_weight, "sp", axis=0, tiled=True),
        lax.all_gather(gate_weight, "sp", axis=0, tiled=True),
        lax.all_gather(out_weight, "sp", axis=1, tiled=True),
    )
    value_all = value_all.reshape(D, LAYERS, channels)
    gate_all = gate_all.reshape(D, LAYERS, channels)
    out_all = out_all.reshape(channels, D, LAYERS)
    earlier = from_behind(stream[-LAYERS * rim_rows :], "sp", 1)
    current = jnp.concatenate([earlier, stream], axis=0)
    for layer_index in range(LAYERS):
        prefix = (LAYERS - layer_index) * rim_rows
        gathered = lax.all_gather(current, "tp", axis=1, tiled=True)
        gathered32 = gathered.astype(jnp.float32)
        scale = lax.rsqrt(jnp.sum(gathered32 * gathered32, axis=1, keepdims=True) / D + EPS)
        run_normed = (gathered32 * scale * norm_gain[layer_index]).astype(jnp.bfloat16)
        value_proj = jnp.dot(
            run_normed, value_all[:, layer_index], preferred_element_type=jnp.float32
        )
        gate_proj = jnp.dot(
            run_normed, gate_all[:, layer_index], preferred_element_type=jnp.float32
        )
        glu_out = value_proj * jax.nn.sigmoid(gate_proj)
        positions = (
            lax.axis_index("sp") * tokens_here - prefix + lax.iota(jnp.int32, current.shape[0])
        )
        extended = jnp.where((positions >= 0)[:, None], glu_out, 0.0)
        residual = current[rim_rows:].astype(jnp.float32)
        conv_out = valid_conv(extended, my_taps[layer_index])
        first_sums, square_sums = lax.psum(
            (jnp.sum(conv_out, axis=1), jnp.sum(conv_out * conv_out, axis=1)), "tp"
        )
        row_mean = (first_sums / C)[:, None]
        row_var = (square_sums / C)[:, None] - row_mean * row_mean
        run_active = jax.nn.silu(
            (conv_out - row_mean) * lax.rsqrt(row_var + EPS) * my_ln_gain[layer_index]
            + my_ln_bias[layer_index]
        ).astype(jnp.bfloat16)
        partial_value = jnp.dot(
            run_active, out_all[:, :, layer_index], preferred_element_type=jnp.float32
        )
        summed = lax.psum_scatter(
            partial_value.astype(jnp.bfloat16), "tp", scatter_dimension=1, tiled=True
        ).astype(jnp.float32)
        current = (residual + summed).astype(jnp.bfloat16)
    final32 = current.astype(jnp.float32)
    squares = lax.psum(jnp.sum(final32 * final32, axis=1), "tp")
    return (final32 * lax.rsqrt(squares[:, None] / D + EPS) * my_final).astype(jnp.bfloat16)


MESH = pl.DeviceIdType.MESH
HALO = 32


def fused_kernel(
    n, x_in, ng_in, v_in, g_in, taps_in, lng_in, lnb_in, o_in, fg_in, out_ref,
    ng_ref, v_ref, g_ref, taps_ref, lng_ref, lnb_ref, o_ref, fg_ref, isem,
    vg, gv, ob, osw, xs, x1, x2, x2r, nb, gl, ext, cv, cvs, cvr, act, st, rst,
    upsem, downsem, sidesem, coresem, xsem, vgsem, osem, swsem, xrsem, x1sem, x2sem, cvsem, glsem, hsem, tsem,
):
    levels = n // 4
    half_levels = levels // 2
    sp = lax.axis_index("sp")
    tp = lax.axis_index("tp")
    z, y, core = sp // 4, (sp // 2) % 2, sp % 2
    peer = 1 - tp
    rows, cols = xs.shape[2], xs.shape[3]
    depth, quarter = vg.shape[1], vg.shape[2] // 2
    width = ob.shape[3]
    has_up, has_down = z < levels - 1, z > 0
    swaps = tp + core == 1
    side, twin = sp + 2 - 4 * y, sp + 1 - 2 * core

    def index(zz, yy, cc):
        return (zz * 2 + yy) * 2 + cc

    loads = [
        pltpu.make_async_copy(source, to, isem.at[i])
        for i, (source, to) in enumerate((
            (v_in, v_ref), (g_in, g_ref), (x_in, xs.at[y, tp]), (o_in, o_ref), (ng_in, ng_ref),
            (taps_in, taps_ref), (lng_in, lng_ref), (lnb_in, lnb_ref), (fg_in, fg_ref)))
    ]
    for load in loads:
        load.start()

    def remote(src, dst, send, recv, to_sp, to_tp):
        return pltpu.make_async_remote_copy(
            src_ref=src, dst_ref=dst, send_sem=send, recv_sem=recv,
            device_id={"sp": to_sp, "tp": to_tp}, device_id_type=MESH)

    def same(ref, send, recv, to_sp):
        return remote(ref, ref, send, recv, to_sp, tp)

    barrier = pltpu.get_barrier_semaphore()

    def greet(to_sp, to_tp):
        pl.semaphore_signal(barrier, inc=1, device_id={"sp": to_sp, "tp": to_tp}, device_id_type=MESH)

    greet(side, tp)
    greet(twin, tp)
    greet(sp, peer)
    pl.when(has_up)(lambda: greet(sp + 4, tp))
    pl.when(has_down)(lambda: greet(sp - 4, tp))
    pl.when(swaps)(lambda: greet(twin, peer))
    before = sp - 1

    @pl.when(sp > 0)
    def _():
        for yy in range(2):
            greet(index(before // 4, yy, before % 2), tp)

    def follows(yy):
        return index(z, yy, core) + 1 < n

    def vg_copy(l, src, send, to_sp):
        return same(vg.at[l * n + src], send, vgsem.at[l, src], to_sp)

    def vg_give(l):
        return remote(gv.at[l], vg.at[l * n + sp], sidesem, vgsem.at[l, sp], side, tp)

    def vg_take(l, src):
        vg_copy(l, src, coresem, twin).wait_recv()

    def vg_up(l, src):
        pl.when(has_up)(lambda: vg_copy(l, src, upsem, sp + 4).start())

    def vg_down(l, src):
        pl.when(has_down)(lambda: vg_copy(l, src, downsem, sp - 4).start())

    def vg_core(l, src):
        vg_copy(l, src, coresem, twin).start()

    def vg_own(l):
        vg_up(l, sp)
        vg_down(l, sp)
        vg_core(l, sp)

    def vg_side(l):
        src = index(z, 1 - y, core)
        vg_take(l, src)
        vg_up(l, src)
        vg_down(l, src)
        vg_core(l, src)

    def vg_line(l, d):
        def one(zz, onward):
            for yy in (y, 1 - y):
                src = index(zz, yy, core)
                vg_take(l, src)
                onward(l, src)
                vg_core(l, src)

        pl.when(z - d >= 0)(lambda: one(z - d, vg_up))
        pl.when(z + d < levels)(lambda: one(z + d, vg_down))

    def vg_other(l):
        for zz in range(levels):
            for yy in range(2):
                vg_take(l, index(zz, yy, 1 - core))

    def o_copy(l, src, send, to_sp):
        return same(ob.at[l, src], send, osem.at[l, src], to_sp)

    def o_swap(l):
        return remote(osw.at[l], ob.at[l, twin], swsem.at[l, 0], swsem.at[l, 1], twin, peer)

    def o_own(l):
        pl.when(swaps)(lambda: o_swap(l).wait_recv())
        pl.when(has_up)(lambda: o_copy(l, sp, upsem, sp + 4).start())
        pl.when(has_down)(lambda: o_copy(l, sp, downsem, sp - 4).start())
        o_copy(l, sp, sidesem, side).start()
        o_copy(l, sp, coresem, twin).start()

    def o_line(l, d):
        def one(zz, up):
            src = index(zz, y, core)
            o_copy(l, src, coresem, twin).wait_recv()
            if up:
                pl.when(has_up)(lambda: o_copy(l, src, upsem, sp + 4).start())
            else:
                pl.when(has_down)(lambda: o_copy(l, src, downsem, sp - 4).start())
            o_copy(l, src, sidesem, side).start()
            o_copy(l, src, coresem, twin).start()

        pl.when(z - d >= 0)(lambda: one(z - d, True))
        pl.when(z + d < levels)(lambda: one(z + d, False))

    def o_across(l, zz):
        src = index(zz, 1 - y, core)
        o_copy(l, src, coresem, twin).wait_recv()
        o_copy(l, src, coresem, twin).start()

    def o_other(l, zz):
        for yy in range(2):
            o_copy(l, index(zz, yy, 1 - core), coresem, twin).wait_recv()

    lo = lax.broadcasted_iota(jnp.int32, (depth, LAYERS * depth), 0)
    hi = lax.broadcasted_iota(jnp.int32, (depth, LAYERS * depth), 1)
    clo = lax.broadcasted_iota(jnp.int32, (LAYERS * width, width), 1)
    chi = lax.broadcasted_iota(jnp.int32, (LAYERS * width, width), 0)

    def pick_rows(l):
        pick = (hi == LAYERS * lo + l).astype(jnp.float32).astype(jnp.bfloat16)
        for yy, keep in ((1 - y, False), (y, True)):
            here = pl.ds(pl.multiple_of(yy * quarter, 128), quarter)
            for kind, ref in enumerate((v_ref, g_ref)):
                picked = jnp.dot(pick, ref[:, here], preferred_element_type=jnp.float32).astype(jnp.bfloat16)
                if keep:
                    vg[l * n + sp, :, kind * quarter : (kind + 1) * quarter] = picked
                else:
                    gv[l, :, kind * quarter : (kind + 1) * quarter] = picked

    def pick_columns(l):
        pick = (chi == LAYERS * clo + l).astype(jnp.float32).astype(jnp.bfloat16)
        picked = jnp.dot(o_ref[...], pick, preferred_element_type=jnp.float32).astype(jnp.bfloat16)

        @pl.when(swaps)
        def _():
            osw[l] = picked
            o_swap(l).start()

        @pl.when(jnp.logical_not(swaps))
        def _():
            ob[l, sp] = picked

    def x_side():
        return same(xs.at[y, tp], sidesem, xrsem.at[0, 0], side)

    def x_peer(yy):
        return remote(xs.at[yy, tp], xs.at[yy, tp], xsem, xrsem.at[yy, 1], sp, peer)

    def square_sum(value):
        return jnp.sum(value * value, axis=1, keepdims=True)

    def normalise_first(yy):
        total = jnp.zeros((rows, 1), jnp.float32)
        for half in range(2):
            total = total + square_sum(xs[yy, half].astype(jnp.float32))
        scale = lax.rsqrt(total / D + EPS)
        for half in range(2):
            gain = ng_ref[0:1, half * cols : (half + 1) * cols]
            nb[yy, :, half * cols : (half + 1) * cols] = (
                xs[yy, half].astype(jnp.float32) * scale * gain).astype(jnp.bfloat16)

    def normalise_next(yy):
        total = jnp.zeros((rows, 1), jnp.float32)
        for half in range(2):
            for zz in range(levels):
                total = total + square_sum(x1[yy, half, zz].astype(jnp.float32))
        scale = lax.rsqrt(total / D + EPS)
        for half in range(2):
            for zz in range(levels):
                for part in range(2):
                    at = index(zz, part, half) * width
                    value = x1[yy, half, zz, :, part * width : (part + 1) * width].astype(jnp.float32)
                    nb[yy, :, at : at + width] = (
                        value * scale * ng_ref[1:2, at : at + width]).astype(jnp.bfloat16)

    def gl_copy(l):
        return remote(gl.at[l, 1 - y], ext.at[l, y, pl.ds(HALO, rows)], sidesem, glsem.at[l], side, tp)

    def halo(l, yy):
        return remote(
            gl.at[l, yy, pl.ds(rows - HALO, HALO)], ext.at[l, y, pl.ds(0, HALO)],
            hsem.at[l, 0, yy], hsem.at[l, 1, y], index(z, yy, core) + 1, tp)

    def halo_wait(l, q):
        remote(
            gl.at[l, 0, pl.ds(rows - HALO, HALO)], ext.at[l, q, pl.ds(0, HALO)],
            hsem.at[l, 0, 0], hsem.at[l, 1, q], side, tp).wait_recv()

    def glu(l):
        both = jnp.dot(
            nb[...].reshape(2 * rows, n * depth), vg[l * n : (l + 1) * n].reshape(n * depth, 2 * quarter),
            preferred_element_type=jnp.float32)
        out = both[:, :quarter] * jax.nn.sigmoid(both[:, quarter:])
        gl[l] = out.reshape(2, rows, quarter)
        for yy in range(2):
            pl.when(follows(yy))(lambda: halo(l, yy).start())
        gl_copy(l).start()
        ext[l, y, HALO:] = gl[l, y]

    def cv_copy(l, q):
        return remote(cvs.at[l, q], cvr.at[l, q], xsem, cvsem.at[l, q], sp, peer)

    def conv_rows(l, q, r0):
        tap_cols = pl.ds(pl.multiple_of((tp * 2 + q) * quarter, 128), quarter)
        running = jnp.zeros((HALO, quarter), jnp.float32)
        for k in range(KW):
            at = r0 + k + HALO - (KW - 1)
            running = running + taps_ref[k, l : l + 1, tap_cols] * ext[l, q, at : at + HALO]
        cv[q, r0 : r0 + HALO] = running
        cvs[l, q, r0 : r0 + HALO] = running.astype(jnp.bfloat16)

    def conv(l):
        for r0 in range(HALO, rows, HALO):
            conv_rows(l, y, r0)
        pl.when(sp > 0)(lambda: halo_wait(l, y))
        conv_rows(l, y, 0)
        cv_copy(l, y).start()
        gl_copy(l).wait_recv()
        for r0 in range(HALO, rows, HALO):
            conv_rows(l, 1 - y, r0)
        pl.when(sp > 0)(lambda: halo_wait(l, 1 - y))
        conv_rows(l, 1 - y, 0)
        cv_copy(l, 1 - y).start()

    def activate(l):
        first = jnp.zeros((rows, 1), jnp.float32)
        second = jnp.zeros((rows, 1), jnp.float32)
        for q in range(2):
            value = cv[q]
            first = first + jnp.sum(value, axis=1, keepdims=True)
            second = second + square_sum(value)
        for q in range(2):
            cv_copy(l, q).wait_recv()
            value = cvr[l, q].astype(jnp.float32)
            first = first + jnp.sum(value, axis=1, keepdims=True)
            second = second + square_sum(value)
        mean = first / C
        scale = lax.rsqrt(second / C - mean * mean + EPS)
        for half, source in ((tp, None), (peer, cvr)):
            for q in range(2):
                value = cv[q] if source is None else source[l, q].astype(jnp.float32)
                here = pl.ds(pl.multiple_of((half * 2 + q) * quarter, 128), quarter)
                v = (value - mean) * scale * lng_ref[l : l + 1, here] + lnb_ref[l : l + 1, here]
                act[half, :, q * quarter : (q + 1) * quarter] = (v / (1.0 + jnp.exp(-v))).astype(jnp.bfloat16)

    def branch(l, zz):
        total = None
        for cc in range(2):
            weights = jnp.concatenate([ob[l, index(zz, 0, cc)], ob[l, index(zz, 1, cc)]], axis=1)
            partial_sum = jnp.dot(act[cc], weights, preferred_element_type=jnp.float32)
            partial_sum = partial_sum.astype(jnp.bfloat16).astype(jnp.float32)
            total = partial_sum if total is None else total + partial_sum
        return total

    def x1_side(zz):
        return same(x1.at[y, tp, zz], sidesem, x1sem.at[0, 0, zz], side)

    def x1_peer(yy, zz):
        return remote(x1.at[yy, tp, zz], x1.at[yy, tp, zz], xsem, x1sem.at[yy, 1, zz], sp, peer)

    def step(i):
        return (z + levels + (1 - 2 * (z // half_levels)) * i) % levels

    def project_first(zz):
        o_across(0, zz)
        o_other(0, zz)
        added = branch(0, zz)
        for part in range(2):
            at = pl.ds(pl.multiple_of((index(zz, part, tp) % (n // 2)) * width, 128), width)
            here = xs[y, zz // half_levels, :, at].astype(jnp.float32)
            x1[y, tp, zz, :, part * width : (part + 1) * width] = (
                here + added[:, part * width : (part + 1) * width]).astype(jnp.bfloat16)
        x1_side(zz).start()
        x1_peer(y, zz).start()

    def x2_copy(zz):
        return remote(x2.at[zz], x2r.at[zz], xsem, x2sem.at[zz % half_levels], sp, peer)

    def project_last(zz):
        fresh = (x1[y, tp, zz].astype(jnp.float32) + branch(1, zz)).astype(jnp.bfloat16)
        x2[zz] = fresh
        pl.when(zz // half_levels == peer)(lambda: x2_copy(zz).start())
        return square_sum(fresh.astype(jnp.float32))

    def stat_copy():
        return remote(st, rst, tsem.at[0], tsem.at[1], sp, peer)

    loads[0].wait()
    loads[1].wait()
    pick_rows(0)

    @pl.when(sp == 0)
    def _():
        for l in range(LAYERS):
            for q in range(2):
                ext[l, q, 0:HALO] = jnp.zeros((HALO, quarter), jnp.float32)

    ends = [has_up, has_down, swaps, follows(0), follows(1)]
    pl.semaphore_wait(barrier, 3 + sum(end.astype(jnp.int32) for end in ends))

    vg_give(0).start()
    vg_own(0)
    loads[2].wait()
    x_peer(y).start()
    x_side().start()
    pick_rows(1)
    vg_give(1).start()
    loads[3].wait()
    for l in range(LAYERS):
        pick_columns(l)
    for load in loads[4:]:
        load.wait()
    vg_side(0)
    for d in range(1, levels - 1):
        vg_line(0, d)
        if d == 1:
            x_peer(y).wait_recv()
            normalise_first(y)
            x_side().wait_recv()
            x_peer(1 - y).start()
    o_own(0)
    vg_line(0, levels - 1)
    x_peer(1 - y).wait_recv()
    normalise_first(1 - y)
    vg_other(0)
    glu(0)
    for d in range(1, levels - 1):
        o_line(0, d)
    vg_own(1)
    vg_side(1)
    conv(0)
    o_line(0, levels - 1)
    activate(0)
    for i in range(levels):
        project_first(step(i))
        if i == 1:
            vg_line(1, 1)
    for d in range(2, levels - 1):
        vg_line(1, d)
    o_own(1)
    for i in range(levels):
        x1_side(step(i)).wait_recv()
        x1_peer(1 - y, step(i)).start()
    for i in range(levels):
        x1_peer(y, step(i)).wait_recv()
    normalise_next(y)
    for i in range(levels):
        x1_peer(1 - y, step(i)).wait_recv()
    normalise_next(1 - y)
    vg_line(1, levels - 1)
    vg_other(1)
    glu(1)
    for d in range(1, levels - 1):
        o_line(1, d)
    conv(1)
    activate(1)
    o_line(1, levels - 1)
    squares = jnp.zeros((rows, 1), jnp.float32)
    for i in range(levels):
        o_across(1, step(i))
        o_other(1, step(i))
        squares = squares + project_last(step(i))
    st[...] = jnp.broadcast_to(squares, (rows, 128)).T[0:8]
    stat_copy().start()

    for zz in range(levels):
        @pl.when(z == zz)
        def _():
            for sem, count in ((upsem, zz + 1 if zz < levels - 1 else 0), (downsem, levels - zz if zz > 0 else 0)):
                if count:
                    block = vg.at[0 : 3 * LAYERS * count]
                    pltpu.make_async_copy(block, block, sem).wait()
    for sem, count in ((coresem, 2 * n), (sidesem, LAYERS + LAYERS * levels + 2 + levels // 2 + LAYERS)):
        block = vg.at[0:count]
        pltpu.make_async_copy(block, block, sem).wait()
    for l in range(LAYERS):
        pl.when(swaps)(lambda: o_swap(l).wait_send())
        for yy in range(2):
            pl.when(follows(yy))(lambda: halo(l, yy).wait_send())

    stat_copy().wait_recv()
    both = st[...] + rst[...]
    total = jnp.concatenate([both] * (128 // 8), axis=0).T[:, 0:1]
    scale = lax.rsqrt(total / D + EPS)
    for i in range(half_levels):
        zz = tp * half_levels + i
        x2_copy(zz).wait_recv()
        for source, parity in ((x2, tp), (x2r, peer)):
            for part in range(2):
                at = ((i * 2 + part) * 2 + parity) * width
                gain = fg_ref[0:1, pl.ds(pl.multiple_of(tp * cols + at, 128), width)]
                value = source[zz, :, part * width : (part + 1) * width].astype(jnp.float32)
                out_ref[:, pl.ds(pl.multiple_of(at, 128), width)] = (value * scale * gain).astype(jnp.bfloat16)
    count = 4 + levels + LAYERS + levels // 4
    block = vg.at[0:count]
    pltpu.make_async_copy(block, block, xsem).wait()
    stat_copy().wait_send()


def fused(n, stream, norm_gain, value_weight, gate_weight, conv_taps, ln_gain, ln_bias, out_weight, final_gain):
    rows, cols = stream.shape
    depth, ch = value_weight.shape[0] // LAYERS, value_weight.shape[1]
    width = out_weight.shape[1] // LAYERS
    levels = n // 4
    bf16, f32 = jnp.bfloat16, jnp.float32
    dma = pltpu.SemaphoreType.DMA
    arrays = (stream, norm_gain, value_weight, gate_weight, conv_taps.transpose(1, 0, 2),
              ln_gain, ln_bias, out_weight, final_gain.reshape(1, -1))
    return pl.pallas_call(
        functools.partial(fused_kernel, n),
        out_shape=jax.ShapeDtypeStruct((rows, cols), bf16),
        in_specs=[pl.BlockSpec(memory_space=pl.ANY)] * 9,
        out_specs=pl.BlockSpec(memory_space=pltpu.VMEM),
        scratch_shapes=[pltpu.VMEM(array.shape, array.dtype) for array in arrays[1:]] + [
            dma((len(arrays),)),
            pltpu.VMEM((LAYERS * n, depth, ch), bf16),
            pltpu.VMEM((LAYERS, depth, ch), bf16),
            pltpu.VMEM((LAYERS, n, ch, width), bf16),
            pltpu.VMEM((LAYERS, ch, width), bf16),
            pltpu.VMEM((2, 2, rows, cols), bf16),
            pltpu.VMEM((2, 2, levels, rows, 2 * width), bf16),
            pltpu.VMEM((levels, rows, 2 * width), bf16),
            pltpu.VMEM((levels, rows, 2 * width), bf16),
            pltpu.VMEM((2, rows, 2 * cols), bf16),
            pltpu.VMEM((LAYERS, 2, rows, ch // 2), f32),
            pltpu.VMEM((LAYERS, 2, HALO + rows, ch // 2), f32),
            pltpu.VMEM((2, rows, ch // 2), f32),
            pltpu.VMEM((LAYERS, 2, rows, ch // 2), bf16),
            pltpu.VMEM((LAYERS, 2, rows, ch // 2), bf16),
            pltpu.VMEM((2, rows, ch), bf16),
            pltpu.VMEM((8, rows), f32),
            pltpu.VMEM((8, rows), f32),
            dma, dma, dma, dma, dma,
            dma((LAYERS, n)),
            dma((LAYERS, n)),
            dma((LAYERS, 2)),
            dma((2, 2)),
            dma((2, 2, levels)),
            dma((levels // 2,)),
            dma((LAYERS, 2)),
            dma((LAYERS,)),
            dma((LAYERS, 2, 2)),
            dma((2,)),
        ],
        compiler_params=pltpu.CompilerParams(collective_id=0, has_side_effects=True),
    )(*arrays)


def solution(mesh):
    placed = (P("sp", "tp"), P(), P("sp", "tp"), P("sp", "tp"), P(), P(), P(), P("tp", "sp"), P())
    n, n_tp = mesh.shape["sp"], mesh.shape["tp"]

    def step(*args):
        stream, out_weight = args[0], args[7]
        fits = (n_tp == 2 and n % 8 == 0 and stream.shape[0] == 128 and out_weight.shape[1] == 128 * LAYERS
                and args[2].shape == (128 * LAYERS, 512))
        return fused(n, *args) if fits else local(*args)

    return jax.shard_map(step, mesh=mesh, in_specs=placed, out_specs=P("sp", "tp"), check_vma=False)
```

time: 93 us -> 77.3 us (0.83)
  the two profiles are of different devices: /device:TPU:4 before, /device:TPU:0 now
where the time goes in v1:
time: 77.3 us; the launch traced here: 77.2 us
  Pallas kernels  75.5 us (98%)
  local copies, waits for them, and re-layouts  1.67 us (2%)
    pallas_call x1, Pallas kernels, fused(): pl.pallas_call(functools.partial(fused_kernel, n), out_shape=jax.ShapeDty...  75.5 us
    unnamed x1, local copies, waits for them, and re-layouts  1.67 us

profile of v1, /device:TPU:0, one launch (start us, length us, event | category | flops | bytes accessed | tf_op | source)
XLA Modules:
  0.0 77.2 jit_solution(12737699836827175235)
XLA Ops:
  0.0 75.5 %shard_map.91 = bf16[128,1024]{1,0:T(8,128)(2,1)} custom-call(bf16[128,1024]{1,0:T(8,128)(2,1)} %x_in.1, f32[2,2048]{1,0:T(2,128)} %ng_in.1, bf16[256,512]{1,0:T(8,128)(2,1)} %v_in.1, bf16[256,512]{1,0:T(8,128)(2,1)} %g_in.1, f32[31,2,1024]{2,1,0:T(2,128)} %bitcast.2, f32[2,1024]{1,0:T(2,128)} %lng_in.1, f32[2,1024]{1,0:T(2,128)} %lnb_in.1, ...), custom_call_target="tpu_custom_call" | custom-call | tf_op jit(solution)/shard_map/pallas_call | solution.py:544
  75.5 1.7 %copy.11 = bf16[128,1024]{1,0:T(8,128)(2,1)} copy(bf16[128,1024]{1,0:T(8,128)(2,1)} %shard_map.91) | data formatting | bytes 524288

commit v2 on v1

--- a/solution.py
+++ b/solution.py
@@ -107,8 +107,8 @@
 def fused_kernel(
     n, x_in, ng_in, v_in, g_in, taps_in, lng_in, lnb_in, o_in, fg_in, out_ref,
     ng_ref, v_ref, g_ref, taps_ref, lng_ref, lnb_ref, o_ref, fg_ref, isem,
-    vg, gv, ob, osw, xs, x1, x2, x2r, nb, gl, ext, cv, cvs, cvr, act, st, rst,
-    upsem, downsem, sidesem, coresem, xsem, vgsem, osem, swsem, xrsem, x1sem, x2sem, cvsem, glsem, hsem, tsem,
+    vg, gv, ob, osw, xs, x1, x2, x2r, nb, gl, gs, gr, ext, cv, cvs, cvr, act, st, rst,
+    upsem, downsem, sidesem, coresem, xsem, gvsem, vgsem, osem, swsem, xrsem, x1sem, x2sem, cvsem, glsem, hsem, tsem,
 ):
     levels = n // 4
     half_levels = levels // 2
@@ -126,6 +126,32 @@
     def index(zz, yy, cc):
         return (zz * 2 + yy) * 2 + cc
 
+    def remote(src, dst, send, recv, to_sp, to_tp):
+        return pltpu.make_async_remote_copy(
+            src_ref=src, dst_ref=dst, send_sem=send, recv_sem=recv,
+            device_id={"sp": to_sp, "tp": to_tp}, device_id_type=MESH)
+
+    def same(ref, send, recv, to_sp):
+        return remote(ref, ref, send, recv, to_sp, tp)
+
+    barrier = pltpu.get_barrier_semaphore()
+
+    def greet(to_sp, to_tp):
+        pl.semaphore_signal(barrier, inc=1, device_id={"sp": to_sp, "tp": to_tp}, device_id_type=MESH)
+
+    greet(side, tp)
+    greet(twin, tp)
+    greet(sp, peer)
+    pl.when(has_up)(lambda: greet(sp + 4, tp))
+    pl.when(has_down)(lambda: greet(sp - 4, tp))
+    pl.when(swaps)(lambda: greet(twin, peer))
+    before = sp - 1
+
+    @pl.when(sp > 0)
+    def _():
+        for yy in range(2):
+            greet(index(before // 4, yy, before % 2), tp)
+
     loads = [
         pltpu.make_async_copy(source, to, isem.at[i])
         for i, (source, to) in enumerate((
@@ -135,40 +161,17 @@
     for load in loads:
         load.start()
 
-    def remote(src, dst, send, recv, to_sp, to_tp):
-        return pltpu.make_async_remote_copy(
-            src_ref=src, dst_ref=dst, send_sem=send, recv_sem=recv,
-            device_id={"sp": to_sp, "tp": to_tp}, device_id_type=MESH)
-
-    def same(ref, send, recv, to_sp):
-        return remote(ref, ref, send, recv, to_sp, tp)
-
-    barrier = pltpu.get_barrier_semaphore()
-
-    def greet(to_sp, to_tp):
-        pl.semaphore_signal(barrier, inc=1, device_id={"sp": to_sp, "tp": to_tp}, device_id_type=MESH)
-
-    greet(side, tp)
-    greet(twin, tp)
-    greet(sp, peer)
-    pl.when(has_up)(lambda: greet(sp + 4, tp))
-    pl.when(has_down)(lambda: greet(sp - 4, tp))
-    pl.when(swaps)(lambda: greet(twin, peer))
-    before = sp - 1
-
-    @pl.when(sp > 0)
-    def _():
-        for yy in range(2):
-            greet(index(before // 4, yy, before % 2), tp)
-
     def follows(yy):
         return index(z, yy, core) + 1 < n
 
     def vg_copy(l, src, send, to_sp):
         return same(vg.at[l * n + src], send, vgsem.at[l, src], to_sp)
 
-    def vg_give(l):
-        return remote(gv.at[l], vg.at[l * n + sp], sidesem, vgsem.at[l, sp], side, tp)
+    def vg_rows(half):
+        return pl.ds(half * (depth // 2), depth // 2)
+
+    def vg_give(l, half):
+        return remote(gv.at[l, vg_rows(half)], vg.at[l * n + sp, vg_rows(half)], sidesem, gvsem.at[l, half], side, tp)
 
     def vg_take(l, src):
         vg_copy(l, src, coresem, twin).wait_recv()
@@ -189,9 +192,11 @@
 
     def vg_side(l):
         src = index(z, 1 - y, core)
-        vg_take(l, src)
-        vg_up(l, src)
-        vg_down(l, src)
+        for half in range(2):
+            vg_give(l, half).wait_recv()
+            block = vg.at[l * n + src, vg_rows(half)]
+            pl.when(has_up)(lambda: same(block, upsem, vgsem.at[l, src], sp + 4).start())
+            pl.when(has_down)(lambda: same(block, downsem, vgsem.at[l, src], sp - 4).start())
         vg_core(l, src)
 
     def vg_line(l, d):
@@ -210,41 +215,56 @@
             for yy in range(2):
                 vg_take(l, index(zz, yy, 1 - core))
 
-    def o_copy(l, src, send, to_sp):
-        return same(ob.at[l, src], send, osem.at[l, src], to_sp)
+    def o_copy(l, src, half, send, to_sp):
+        block = ob.at[l, src, pl.ds(half * (ob.shape[2] // 2), ob.shape[2] // 2)]
+        return same(block, send, osem.at[l, src, half], to_sp)
 
     def o_swap(l):
         return remote(osw.at[l], ob.at[l, twin], swsem.at[l, 0], swsem.at[l, 1], twin, peer)
 
-    def o_own(l):
-        pl.when(swaps)(lambda: o_swap(l).wait_recv())
-        pl.when(has_up)(lambda: o_copy(l, sp, upsem, sp + 4).start())
-        pl.when(has_down)(lambda: o_copy(l, sp, downsem, sp - 4).start())
-        o_copy(l, sp, sidesem, side).start()
-        o_copy(l, sp, coresem, twin).start()
+    def o_take(l, src, half):
+        o_copy(l, src, half, coresem, twin).wait_recv()
+
+    def o_up(l, src, half):
+        pl.when(has_up)(lambda: o_copy(l, src, half, upsem, sp + 4).start())
+
+    def o_down(l, src, half):
+        pl.when(has_down)(lambda: o_copy(l, src, half, downsem, sp - 4).start())
+
+    def o_here(l, src, half):
+        o_copy(l, src, half, sidesem, side).start()
+        o_copy(l, src, half, coresem, twin).start()
+
+    def o_own_line(l):
+        for half in range(2):
+            o_up(l, sp, half)
+            o_down(l, sp, half)
+
+    def o_own_here(l):
+        for half in range(2):
+            o_here(l, sp, half)
 
     def o_line(l, d):
-        def one(zz, up):
+        def one(zz, onward):
             src = index(zz, y, core)
-            o_copy(l, src, coresem, twin).wait_recv()
-            if up:
-                pl.when(has_up)(lambda: o_copy(l, src, upsem, sp + 4).start())
-            else:
-                pl.when(has_down)(lambda: o_copy(l, src, downsem, sp - 4).start())
-            o_copy(l, src, sidesem, side).start()
-            o_copy(l, src, coresem, twin).start()
-
-        pl.when(z - d >= 0)(lambda: one(z - d, True))
-        pl.when(z + d < levels)(lambda: one(z + d, False))
+            for half in range(2):
+                o_take(l, src, half)
+                onward(l, src, half)
+                o_here(l, src, half)
+
+        pl.when(z - d >= 0)(lambda: one(z - d, o_up))
+        pl.when(z + d < levels)(lambda: one(z + d, o_down))
 
     def o_across(l, zz):
         src = index(zz, 1 - y, core)
-        o_copy(l, src, coresem, twin).wait_recv()
-        o_copy(l, src, coresem, twin).start()
+        for half in range(2):
+            o_take(l, src, half)
+            o_copy(l, src, half, coresem, twin).start()
 
     def o_other(l, zz):
         for yy in range(2):
-            o_copy(l, index(zz, yy, 1 - core), coresem, twin).wait_recv()
+            for half in range(2):
+                o_take(l, index(zz, yy, 1 - core), half)
 
     lo = lax.broadcasted_iota(jnp.int32, (depth, LAYERS * depth), 0)
     hi = lax.broadcasted_iota(jnp.int32, (depth, LAYERS * depth), 1)
@@ -309,7 +329,7 @@
                         value * scale * ng_ref[1:2, at : at + width]).astype(jnp.bfloat16)
 
     def gl_copy(l):
-        return remote(gl.at[l, 1 - y], ext.at[l, y, pl.ds(HALO, rows)], sidesem, glsem.at[l], side, tp)
+        return remote(gs.at[l], gr.at[l], sidesem, glsem.at[l], side, tp)
 
     def halo(l, yy):
         return remote(
@@ -329,11 +349,13 @@
         gl[l] = out.reshape(2, rows, quarter)
         for yy in range(2):
             pl.when(follows(yy))(lambda: halo(l, yy).start())
+        gs[l] = gl[l, 1 - y].astype(jnp.bfloat16)
         gl_copy(l).start()
         ext[l, y, HALO:] = gl[l, y]
 
-    def cv_copy(l, q):
-        return remote(cvs.at[l, q], cvr.at[l, q], xsem, cvsem.at[l, q], sp, peer)
+    def cv_copy(l, q, half):
+        here = pl.ds(half * (rows // 2), rows // 2)
+        return remote(cvs.at[l, q, here], cvr.at[l, q, here], xsem, cvsem.at[l, q, half], sp, peer)
 
     def conv_rows(l, q, r0):
         tap_cols = pl.ds(pl.multiple_of((tp * 2 + q) * quarter, 128), quarter)
@@ -344,20 +366,20 @@
         cv[q, r0 : r0 + HALO] = running
         cvs[l, q, r0 : r0 + HALO] = running.astype(jnp.bfloat16)
 
-    def conv(l):
-        for r0 in range(HALO, rows, HALO):
-            conv_rows(l, y, r0)
-        pl.when(sp > 0)(lambda: halo_wait(l, y))
-        conv_rows(l, y, 0)
-        cv_copy(l, y).start()
+    def conv(l, q):
+        for half in (1, 0):
+            for r0 in range(half * rows // 2 + (HALO if half == 0 else 0), (half + 1) * rows // 2, HALO):
+                conv_rows(l, q, r0)
+            if half == 0:
+                pl.when(sp > 0)(lambda: halo_wait(l, q))
+                conv_rows(l, q, 0)
+            cv_copy(l, q, half).start()
+
+    def take_glu(l):
         gl_copy(l).wait_recv()
-        for r0 in range(HALO, rows, HALO):
-            conv_rows(l, 1 - y, r0)
-        pl.when(sp > 0)(lambda: halo_wait(l, 1 - y))
-        conv_rows(l, 1 - y, 0)
-        cv_copy(l, 1 - y).start()
-
-    def activate(l):
+        ext[l, 1 - y, HALO:] = gr[l].astype(jnp.float32)
+
+    def activate(l, between):
         first = jnp.zeros((rows, 1), jnp.float32)
         second = jnp.zeros((rows, 1), jnp.float32)
         for q in range(2):
@@ -365,7 +387,10 @@
             first = first + jnp.sum(value, axis=1, keepdims=True)
             second = second + square_sum(value)
         for q in range(2):
-            cv_copy(l, q).wait_recv()
+            for half in range(2):
+                cv_copy(l, q, half).wait_recv()
+        between()
+        for q in range(2):
             value = cvr[l, q].astype(jnp.float32)
             first = first + jnp.sum(value, axis=1, keepdims=True)
             second = second + square_sum(value)
@@ -393,11 +418,13 @@
     def x1_peer(yy, zz):
         return remote(x1.at[yy, tp, zz], x1.at[yy, tp, zz], xsem, x1sem.at[yy, 1, zz], sp, peer)
 
+    def x1_diagonal(zz):
+        return same(x1.at[y, peer, zz], sidesem, x1sem.at[1, 0, zz], side)
+
     def step(i):
         return (z + levels + (1 - 2 * (z // half_levels)) * i) % levels
 
     def project_first(zz):
-        o_across(0, zz)
         o_other(0, zz)
         added = branch(0, zz)
         for part in range(2):
@@ -433,16 +460,20 @@
     ends = [has_up, has_down, swaps, follows(0), follows(1)]
     pl.semaphore_wait(barrier, 3 + sum(end.astype(jnp.int32) for end in ends))
 
-    vg_give(0).start()
+    for half in range(2):
+        vg_give(0, half).start()
     vg_own(0)
     loads[2].wait()
     x_peer(y).start()
     x_side().start()
     pick_rows(1)
-    vg_give(1).start()
+    for half in range(2):
+        vg_give(1, half).start()
     loads[3].wait()
     for l in range(LAYERS):
         pick_columns(l)
+    keeps = jnp.logical_not(swaps)
+    pl.when(keeps)(lambda: o_own_line(0))
     for load in loads[4:]:
         load.wait()
     vg_side(0)
@@ -453,46 +484,86 @@
             normalise_first(y)
             x_side().wait_recv()
             x_peer(1 - y).start()
-    o_own(0)
+    @pl.when(swaps)
+    def _():
+        o_swap(0).wait_recv()
+        o_own_line(0)
+
+    o_own_here(0)
     vg_line(0, levels - 1)
     x_peer(1 - y).wait_recv()
     normalise_first(1 - y)
     vg_other(0)
     glu(0)
-    for d in range(1, levels - 1):
-        o_line(0, d)
+    middle = jnp.logical_and(has_up, has_down)
+    last = jnp.logical_not(middle)
+
+    def o_near(l, *distances):
+        for d in distances:
+            o_line(l, d)
+
+    pl.when(middle)(lambda: o_near(0, *range(1, levels - 1)))
     vg_own(1)
     vg_side(1)
-    conv(0)
-    o_line(0, levels - 1)
-    activate(0)
+    conv(0, y)
+    pl.when(last)(lambda: o_near(0, 1))
+    take_glu(0)
+    conv(0, 1 - y)
+    o_across(0, step(0))
+    pl.when(last)(lambda: o_near(0, *range(2, levels - 1)))
+
+    def between(l):
+        o_line(l, levels - 1)
+        o_across(l, step(1))
+
+    activate(0, lambda: between(0))
+    project_first(step(0))
+    o_across(0, step(2))
+    project_first(step(1))
+    pl.when(middle)(lambda: vg_line(1, 1))
+    for i in range(2, levels):
+        if i > 2:
+            o_across(0, step(i))
+        project_first(step(i))
+    pl.when(last)(lambda: vg_line(1, 1))
     for i in range(levels):
-        project_first(step(i))
-        if i == 1:
-            vg_line(1, 1)
+        x1_side(step(i)).wait_recv()
+        if i % 2 == 0:
+            x1_peer(1 - y, step(i)).start()
+        x1_peer(y, step(i)).wait_recv()
+        if i % 2 == 1:
+            x1_diagonal(step(i)).start()
     for d in range(2, levels - 1):
         vg_line(1, d)
-    o_own(1)
+    normalise_next(y)
+
+    @pl.when(swaps)
+    def _():
+        o_swap(1).wait_recv()
+
+    o_own_line(1)
+    o_own_here(1)
     for i in range(levels):
-        x1_side(step(i)).wait_recv()
-        x1_peer(1 - y, step(i)).start()
-    for i in range(levels):
-        x1_peer(y, step(i)).wait_recv()
-    normalise_next(y)
-    for i in range(levels):
-        x1_peer(1 - y, step(i)).wait_recv()
+        if i % 2 == 0:
+            x1_peer(1 - y, step(i)).wait_recv()
+        else:
+            x1_diagonal(step(i)).wait_recv()
     normalise_next(1 - y)
     vg_line(1, levels - 1)
     vg_other(1)
     glu(1)
-    for d in range(1, levels - 1):
-        o_line(1, d)
-    conv(1)
-    activate(1)
-    o_line(1, levels - 1)
+    pl.when(middle)(lambda: o_near(1, *range(1, levels - 1)))
+    conv(1, y)
+    pl.when(last)(lambda: o_near(1, 1))
+    take_glu(1)
+    conv(1, 1 - y)
+    o_across(1, step(0))
+    pl.when(last)(lambda: o_near(1, *range(2, levels - 1)))
+    activate(1, lambda: between(1))
     squares = jnp.zeros((rows, 1), jnp.float32)
     for i in range(levels):
-        o_across(1, step(i))
+        if i > 0 and i < levels - 1:
+            o_across(1, step(i + 1))
         o_other(1, step(i))
         squares = squares + project_last(step(i))
     st[...] = jnp.broadcast_to(squares, (rows, 128)).T[0:8]
@@ -505,7 +576,7 @@
                 if count:
                     block = vg.at[0 : 3 * LAYERS * count]
                     pltpu.make_async_copy(block, block, sem).wait()
-    for sem, count in ((coresem, 2 * n), (sidesem, LAYERS + LAYERS * levels + 2 + levels // 2 + LAYERS)):
+    for sem, count in ((coresem, 2 * n), (sidesem, LAYERS + LAYERS * levels + 2 + levels // 2 + levels // 4 + LAYERS // 2)):
         block = vg.at[0:count]
         pltpu.make_async_copy(block, block, sem).wait()
     for l in range(LAYERS):
@@ -526,7 +597,7 @@
                 gain = fg_ref[0:1, pl.ds(pl.multiple_of(tp * cols + at, 128), width)]
                 value = source[zz, :, part * width : (part + 1) * width].astype(jnp.float32)
                 out_ref[:, pl.ds(pl.multiple_of(at, 128), width)] = (value * scale * gain).astype(jnp.bfloat16)
-    count = 4 + levels + LAYERS + levels // 4
+    count = 4 + levels // 2 + levels // 4 + LAYERS + levels // 4
     block = vg.at[0:count]
     pltpu.make_async_copy(block, block, xsem).wait()
     stat_copy().wait_send()
@@ -543,7 +614,7 @@
               ln_gain, ln_bias, out_weight, final_gain.reshape(1, -1))
     return pl.pallas_call(
         functools.partial(fused_kernel, n),
-        out_shape=jax.ShapeDtypeStruct((rows, cols), bf16),
+        out_shape=pltpu.VMEM((rows, cols), bf16),
         in_specs=[pl.BlockSpec(memory_space=pl.ANY)] * 9,
         out_specs=pl.BlockSpec(memory_space=pltpu.VMEM),
         scratch_shapes=[pltpu.VMEM(array.shape, array.dtype) for array in arrays[1:]] + [
@@ -558,6 +629,8 @@
             pltpu.VMEM((levels, rows, 2 * width), bf16),
             pltpu.VMEM((2, rows, 2 * cols), bf16),
             pltpu.VMEM((LAYERS, 2, rows, ch // 2), f32),
+            pltpu.VMEM((LAYERS, rows, ch // 2), bf16),
+            pltpu.VMEM((LAYERS, rows, ch // 2), bf16),
             pltpu.VMEM((LAYERS, 2, HALO + rows, ch // 2), f32),
             pltpu.VMEM((2, rows, ch // 2), f32),
             pltpu.VMEM((LAYERS, 2, rows, ch // 2), bf16),
@@ -566,13 +639,14 @@
             pltpu.VMEM((8, rows), f32),
             pltpu.VMEM((8, rows), f32),
             dma, dma, dma, dma, dma,
+            dma((LAYERS, 2)),
             dma((LAYERS, n)),
-            dma((LAYERS, n)),
+            dma((LAYERS, n, 2)),
             dma((LAYERS, 2)),
             dma((2, 2)),
             dma((2, 2, levels)),
             dma((levels // 2,)),
-            dma((LAYERS, 2)),
+            dma((LAYERS, 2, 2)),
             dma((LAYERS,)),
             dma((LAYERS, 2, 2)),
             dma((2,)),

time: 77.3 us -> 71.8 us (0.929)
  Pallas kernels: 75.5 us -> 70.9 us
  local copies, waits for them, and re-layouts: 1.67 us -> 0.71 us
    pallas_call x1, Pallas kernels: 75.5 us -> 70.9 us  [fused(): pl.pallas_call(functools.partial(fused_kernel, n), out_shape=pltpu.VMEM((...]
    unnamed x1, local copies, waits for them, and re-layouts: 1.67 us -> 0.71 us
where the time goes in v2:
time: 71.8 us; the launch traced here: 71.6 us
  Pallas kernels  70.9 us (99%)
    pallas_call x1, Pallas kernels, fused(): pl.pallas_call(functools.partial(fused_kernel, n), out_shape=pltpu.VMEM((...  70.9 us

profile of v2, /device:TPU:0, one launch (start us, length us, event | category | flops | bytes accessed | tf_op | source)
XLA Modules:
  0.0 71.6 jit_solution(1395630154500928655)
XLA Ops:
  0.0 70.9 %shard_map.91 = bf16[128,1024]{1,0:T(8,128)(2,1)S(1)} custom-call(bf16[128,1024]{1,0:T(8,128)(2,1)} %x_in.1, f32[2,2048]{1,0:T(2,128)} %ng_in.1, bf16[256,512]{1,0:T(8,128)(2,1)} %v_in.1, bf16[256,512]{1,0:T(8,128)(2,1)} %g_in.1, f32[31,2,1024]{2,1,0:T(2,128)} %bitcast.2, f32[2,1024]{1,0:T(2,128)} %lng_in.1, f32[2,1024]{1,0:T(2,128)} %lnb_in.1, ...), custom_call_target="tpu_custom_call" | custom-call | tf_op jit(solution)/shard_map/pallas_call | solution.py:615
  70.9 0.7 copy.11

commit v3 on v2

--- a/solution.py
+++ b/solution.py
@@ -108,7 +108,7 @@
     n, x_in, ng_in, v_in, g_in, taps_in, lng_in, lnb_in, o_in, fg_in, out_ref,
     ng_ref, v_ref, g_ref, taps_ref, lng_ref, lnb_ref, o_ref, fg_ref, isem,
     vg, gv, ob, osw, xs, x1, x2, x2r, nb, gl, gs, gr, ext, cv, cvs, cvr, act, st, rst,
-    upsem, downsem, sidesem, coresem, xsem, gvsem, vgsem, osem, swsem, xrsem, x1sem, x2sem, cvsem, glsem, hsem, tsem,
+    upsem, downsem, sidesem, coresem, xsem, gvsem, vgsem, vcsem, osem, ocsem, swsem, xrsem, x1sem, x2sem, cvsem, glsem, hssem, hsem, tsem,
 ):
     levels = n // 4
     half_levels = levels // 2
@@ -126,6 +126,9 @@
     def index(zz, yy, cc):
         return (zz * 2 + yy) * 2 + cc
 
+    def landed(block, sem):
+        pltpu.make_async_copy(block, block, sem).wait()
+
     def remote(src, dst, send, recv, to_sp, to_tp):
         return pltpu.make_async_remote_copy(
             src_ref=src, dst_ref=dst, send_sem=send, recv_sem=recv,
@@ -153,7 +156,7 @@
             greet(index(before // 4, yy, before % 2), tp)
 
     loads = [
-        pltpu.make_async_copy(source, to, isem.at[i])
+        pltpu.make_async_copy(source, to, isem.at[max(i - 1, 0)])
         for i, (source, to) in enumerate((
             (v_in, v_ref), (g_in, g_ref), (x_in, xs.at[y, tp]), (o_in, o_ref), (ng_in, ng_ref),
             (taps_in, taps_ref), (lng_in, lng_ref), (lnb_in, lnb_ref), (fg_in, fg_ref)))
@@ -165,13 +168,18 @@
         return index(z, yy, core) + 1 < n
 
     def vg_copy(l, src, send, to_sp):
-        return same(vg.at[l * n + src], send, vgsem.at[l, src], to_sp)
-
-    def vg_rows(half):
-        return pl.ds(half * (depth // 2), depth // 2)
+        return same(vg.at[l * n + src], send, vgsem.at[l, src // 2], to_sp)
+
+    def gives(l):
+        return 2 if l == 0 else 1
+
+    def vg_rows(l, half):
+        return pl.ds(half * (depth // gives(l)), depth // gives(l))
 
     def vg_give(l, half):
-        return remote(gv.at[l, vg_rows(half)], vg.at[l * n + sp, vg_rows(half)], sidesem, gvsem.at[l, half], side, tp)
+        here = vg_rows(l, half)
+        return remote(
+            gv.at[l, here], vg.at[l * n + sp, here], sidesem, gvsem.at[half if l == 0 else l + 1], side, tp)
 
     def vg_take(l, src):
         vg_copy(l, src, coresem, twin).wait_recv()
@@ -183,7 +191,7 @@
         pl.when(has_down)(lambda: vg_copy(l, src, downsem, sp - 4).start())
 
     def vg_core(l, src):
-        vg_copy(l, src, coresem, twin).start()
+        same(vg.at[l * n + src], coresem, vcsem.at[l], twin).start()
 
     def vg_own(l):
         vg_up(l, sp)
@@ -192,11 +200,11 @@
 
     def vg_side(l):
         src = index(z, 1 - y, core)
-        for half in range(2):
+        for half in range(gives(l)):
             vg_give(l, half).wait_recv()
-            block = vg.at[l * n + src, vg_rows(half)]
-            pl.when(has_up)(lambda: same(block, upsem, vgsem.at[l, src], sp + 4).start())
-            pl.when(has_down)(lambda: same(block, downsem, vgsem.at[l, src], sp - 4).start())
+            block = vg.at[l * n + src, vg_rows(l, half)]
+            pl.when(has_up)(lambda: same(block, upsem, vgsem.at[l, src // 2], sp + 4).start())
+            pl.when(has_down)(lambda: same(block, downsem, vgsem.at[l, src // 2], sp - 4).start())
         vg_core(l, src)
 
     def vg_line(l, d):
@@ -211,19 +219,28 @@
         pl.when(z + d < levels)(lambda: one(z + d, vg_down))
 
     def vg_other(l):
-        for zz in range(levels):
-            for yy in range(2):
-                vg_take(l, index(zz, yy, 1 - core))
+        landed(vg.at[0 : n // 2], vcsem.at[l])
+
+    def halves(l):
+        return range(2 if l == LAYERS - 1 else 1)
+
+    def o_block(l, src, half):
+        size = ob.shape[2] // len(halves(l))
+        return ob.at[l, src, pl.ds(half * size, size)]
 
     def o_copy(l, src, half, send, to_sp):
-        block = ob.at[l, src, pl.ds(half * (ob.shape[2] // 2), ob.shape[2] // 2)]
-        return same(block, send, osem.at[l, src, half], to_sp)
+        at = src // 2 if l == 0 else n // 2 + src // 2 * 2 + half
+        return same(o_block(l, src, half), send, osem.at[at], to_sp)
+
+    def o_core(l, src, half):
+        at = src // 4 if l == 0 else levels + src // 2
+        same(o_block(l, src, half), coresem, ocsem.at[at], twin).start()
 
     def o_swap(l):
-        return remote(osw.at[l], ob.at[l, twin], swsem.at[l, 0], swsem.at[l, 1], twin, peer)
+        return remote(osw.at[l], ob.at[l, twin], swsem.at[0], swsem.at[1 + l], twin, peer)
 
     def o_take(l, src, half):
-        o_copy(l, src, half, coresem, twin).wait_recv()
+        o_copy(l, src, half, sidesem, side).wait_recv()
 
     def o_up(l, src, half):
         pl.when(has_up)(lambda: o_copy(l, src, half, upsem, sp + 4).start())
@@ -233,21 +250,24 @@
 
     def o_here(l, src, half):
         o_copy(l, src, half, sidesem, side).start()
-        o_copy(l, src, half, coresem, twin).start()
-
-    def o_own_line(l):
-        for half in range(2):
-            o_up(l, sp, half)
-            o_down(l, sp, half)
+        o_core(l, src, half)
+
+    def o_swapped(l):
+        pl.when(swaps)(lambda: o_swap(l).wait_recv())
+
+    def o_own_line(l, up, down):
+        for half in halves(l):
+            pl.when(up)(lambda: o_up(l, sp, half))
+            pl.when(down)(lambda: o_down(l, sp, half))
 
     def o_own_here(l):
-        for half in range(2):
+        for half in halves(l):
             o_here(l, sp, half)
 
     def o_line(l, d):
         def one(zz, onward):
             src = index(zz, y, core)
-            for half in range(2):
+            for half in halves(l):
                 o_take(l, src, half)
                 onward(l, src, half)
                 o_here(l, src, half)
@@ -257,14 +277,15 @@
 
     def o_across(l, zz):
         src = index(zz, 1 - y, core)
-        for half in range(2):
+        for half in halves(l):
             o_take(l, src, half)
-            o_copy(l, src, half, coresem, twin).start()
-
-    def o_other(l, zz):
-        for yy in range(2):
-            for half in range(2):
-                o_take(l, index(zz, yy, 1 - core), half)
+            o_core(l, src, half)
+
+    def o_other_both(zz):
+        landed(ob.at[0, 0:2], ocsem.at[zz])
+
+    def o_other(zz, yy):
+        landed(ob.at[0, 0], ocsem.at[levels + zz * 2 + yy])
 
     lo = lax.broadcasted_iota(jnp.int32, (depth, LAYERS * depth), 0)
     hi = lax.broadcasted_iota(jnp.int32, (depth, LAYERS * depth), 1)
@@ -277,10 +298,11 @@
             here = pl.ds(pl.multiple_of(yy * quarter, 128), quarter)
             for kind, ref in enumerate((v_ref, g_ref)):
                 picked = jnp.dot(pick, ref[:, here], preferred_element_type=jnp.float32).astype(jnp.bfloat16)
+                at = kind * quarter
                 if keep:
-                    vg[l * n + sp, :, kind * quarter : (kind + 1) * quarter] = picked
+                    vg[l * n + sp, :, at : at + quarter] = picked
                 else:
-                    gv[l, :, kind * quarter : (kind + 1) * quarter] = picked
+                    gv[l, :, at : at + quarter] = picked
 
     def pick_columns(l):
         pick = (chi == LAYERS * clo + l).astype(jnp.float32).astype(jnp.bfloat16)
@@ -296,10 +318,11 @@
             ob[l, sp] = picked
 
     def x_side():
-        return same(xs.at[y, tp], sidesem, xrsem.at[0, 0], side)
-
-    def x_peer(yy):
-        return remote(xs.at[yy, tp], xs.at[yy, tp], xsem, xrsem.at[yy, 1], sp, peer)
+        return same(xs.at[y, tp], sidesem, xrsem.at[0], side)
+
+    def x_peer(far):
+        block = xs.at[1 - y if far else y, tp]
+        return remote(block, block, xsem, xrsem.at[1 + far], sp, peer)
 
     def square_sum(value):
         return jnp.sum(value * value, axis=1, keepdims=True)
@@ -318,44 +341,52 @@
         total = jnp.zeros((rows, 1), jnp.float32)
         for half in range(2):
             for zz in range(levels):
-                total = total + square_sum(x1[yy, half, zz].astype(jnp.float32))
+                for part in range(2):
+                    total = total + square_sum(x1[yy, half, zz, part].astype(jnp.float32))
         scale = lax.rsqrt(total / D + EPS)
         for half in range(2):
             for zz in range(levels):
                 for part in range(2):
                     at = index(zz, part, half) * width
-                    value = x1[yy, half, zz, :, part * width : (part + 1) * width].astype(jnp.float32)
+                    value = x1[yy, half, zz, part].astype(jnp.float32)
                     nb[yy, :, at : at + width] = (
                         value * scale * ng_ref[1:2, at : at + width]).astype(jnp.bfloat16)
 
-    def gl_copy(l):
-        return remote(gs.at[l], gr.at[l], sidesem, glsem.at[l], side, tp)
+    def gl_copy(l, half):
+        here = pl.ds(half * (rows // 2), rows // 2)
+        return remote(gs.at[l, here], gr.at[l, here], sidesem, glsem.at[l], side, tp)
 
     def halo(l, yy):
         return remote(
-            gl.at[l, yy, pl.ds(rows - HALO, HALO)], ext.at[l, y, pl.ds(0, HALO)],
-            hsem.at[l, 0, yy], hsem.at[l, 1, y], index(z, yy, core) + 1, tp)
+            gl.at[l, yy], ext.at[l, y, pl.ds(0, HALO)],
+            hssem.at[yy], hsem.at[l, y], index(z, yy, core) + 1, tp)
 
     def halo_wait(l, q):
         remote(
-            gl.at[l, 0, pl.ds(rows - HALO, HALO)], ext.at[l, q, pl.ds(0, HALO)],
-            hsem.at[l, 0, 0], hsem.at[l, 1, q], side, tp).wait_recv()
+            gl.at[l, 0], ext.at[l, q, pl.ds(0, HALO)],
+            hssem.at[0], hsem.at[l, q], side, tp).wait_recv()
 
     def glu(l):
-        both = jnp.dot(
-            nb[...].reshape(2 * rows, n * depth), vg[l * n : (l + 1) * n].reshape(n * depth, 2 * quarter),
-            preferred_element_type=jnp.float32)
-        out = both[:, :quarter] * jax.nn.sigmoid(both[:, quarter:])
-        gl[l] = out.reshape(2, rows, quarter)
-        for yy in range(2):
-            pl.when(follows(yy))(lambda: halo(l, yy).start())
-        gs[l] = gl[l, 1 - y].astype(jnp.bfloat16)
-        gl_copy(l).start()
-        ext[l, y, HALO:] = gl[l, y]
+        weights = vg[l * n : (l + 1) * n].reshape(n * depth, 2 * quarter)
+
+        def tokens(yy):
+            both = jnp.dot(nb[yy], weights, preferred_element_type=jnp.float32)
+            return both[:, :quarter] * jax.nn.sigmoid(both[:, quarter:])
+
+        theirs = tokens(1 - y)
+        gs[l] = theirs.astype(jnp.bfloat16)
+        gl[l, 1 - y] = theirs[rows - HALO :]
+        for half in (1, 0):
+            gl_copy(l, half).start()
+        pl.when(follows(1 - y))(lambda: halo(l, 1 - y).start())
+        mine = tokens(y)
+        ext[l, y, HALO:] = mine
+        gl[l, y] = mine[rows - HALO :]
+        pl.when(follows(y))(lambda: halo(l, y).start())
 
     def cv_copy(l, q, half):
         here = pl.ds(half * (rows // 2), rows // 2)
-        return remote(cvs.at[l, q, here], cvr.at[l, q, here], xsem, cvsem.at[l, q, half], sp, peer)
+        return remote(cvs.at[l, q, here], cvr.at[l, q, here], xsem, cvsem.at[l], sp, peer)
 
     def conv_rows(l, q, r0):
         tap_cols = pl.ds(pl.multiple_of((tp * 2 + q) * quarter, 128), quarter)
@@ -376,7 +407,7 @@
             cv_copy(l, q, half).start()
 
     def take_glu(l):
-        gl_copy(l).wait_recv()
+        landed(gr.at[l], glsem.at[l])
         ext[l, 1 - y, HALO:] = gr[l].astype(jnp.float32)
 
     def activate(l, between):
@@ -386,9 +417,7 @@
             value = cv[q]
             first = first + jnp.sum(value, axis=1, keepdims=True)
             second = second + square_sum(value)
-        for q in range(2):
-            for half in range(2):
-                cv_copy(l, q, half).wait_recv()
+        landed(cvr.at[l], cvsem.at[l])
         between()
         for q in range(2):
             value = cvr[l, q].astype(jnp.float32)
@@ -413,42 +442,63 @@
         return total
 
     def x1_side(zz):
-        return same(x1.at[y, tp, zz], sidesem, x1sem.at[0, 0, zz], side)
-
-    def x1_peer(yy, zz):
-        return remote(x1.at[yy, tp, zz], x1.at[yy, tp, zz], xsem, x1sem.at[yy, 1, zz], sp, peer)
+        return same(x1.at[y, tp, zz], sidesem, x1sem.at[0, zz], side)
+
+    def x1_peer(far, zz):
+        block = x1.at[1 - y if far else y, tp, zz]
+        return remote(block, block, xsem, x1sem.at[1 + far, zz], sp, peer)
 
     def x1_diagonal(zz):
-        return same(x1.at[y, peer, zz], sidesem, x1sem.at[1, 0, zz], side)
+        return same(x1.at[y, peer, zz], sidesem, x1sem.at[2, zz], side)
 
     def step(i):
         return (z + levels + (1 - 2 * (z // half_levels)) * i) % levels
 
     def project_first(zz):
-        o_other(0, zz)
+        o_other_both(zz)
         added = branch(0, zz)
         for part in range(2):
             at = pl.ds(pl.multiple_of((index(zz, part, tp) % (n // 2)) * width, 128), width)
             here = xs[y, zz // half_levels, :, at].astype(jnp.float32)
-            x1[y, tp, zz, :, part * width : (part + 1) * width] = (
+            x1[y, tp, zz, part] = (
                 here + added[:, part * width : (part + 1) * width]).astype(jnp.bfloat16)
         x1_side(zz).start()
-        x1_peer(y, zz).start()
-
-    def x2_copy(zz):
-        return remote(x2.at[zz], x2r.at[zz], xsem, x2sem.at[zz % half_levels], sp, peer)
+        x1_peer(0, zz).start()
+
+    def x2_copy(zz, part):
+        return remote(x2.at[zz, part], x2r.at[zz, part], xsem, x2sem, sp, peer)
+
+    def put_last(zz, part, added):
+        fresh = (x1[y, tp, zz, part].astype(jnp.float32) + added).astype(jnp.bfloat16)
+        x2[zz, part] = fresh
+        pl.when(zz // half_levels == peer)(lambda: x2_copy(zz, part).start())
+        return square_sum(fresh.astype(jnp.float32))
 
     def project_last(zz):
-        fresh = (x1[y, tp, zz].astype(jnp.float32) + branch(1, zz)).astype(jnp.bfloat16)
-        x2[zz] = fresh
-        pl.when(zz // half_levels == peer)(lambda: x2_copy(zz).start())
-        return square_sum(fresh.astype(jnp.float32))
+        o_other(zz, y)
+        o_other(zz, 1 - y)
+        added = branch(1, zz)
+        return put_last(zz, 0, added[:, :width]) + put_last(zz, 1, added[:, width:])
+
+    def project_end(zz):
+        total = None
+        for part in (y, 1 - y):
+            if total is not None:
+                o_across(1, zz)
+            o_other(zz, part)
+            added = None
+            for cc in range(2):
+                one = jnp.dot(act[cc], ob[1, index(zz, part, cc)], preferred_element_type=jnp.float32)
+                one = one.astype(jnp.bfloat16).astype(jnp.float32)
+                added = one if added is None else added + one
+            one = put_last(zz, part, added)
+            total = one if total is None else total + one
+        return total
 
     def stat_copy():
         return remote(st, rst, tsem.at[0], tsem.at[1], sp, peer)
 
-    loads[0].wait()
-    loads[1].wait()
+    landed(vg.at[0 : 2 * LAYERS], isem.at[0])
     pick_rows(0)
 
     @pl.when(sp == 0)
@@ -460,49 +510,49 @@
     ends = [has_up, has_down, swaps, follows(0), follows(1)]
     pl.semaphore_wait(barrier, 3 + sum(end.astype(jnp.int32) for end in ends))
 
-    for half in range(2):
+    for half in range(gives(0)):
         vg_give(0, half).start()
     vg_own(0)
     loads[2].wait()
-    x_peer(y).start()
+    x_peer(0).start()
     x_side().start()
     pick_rows(1)
-    for half in range(2):
+    for half in range(gives(1)):
         vg_give(1, half).start()
     loads[3].wait()
     for l in range(LAYERS):
         pick_columns(l)
-    keeps = jnp.logical_not(swaps)
-    pl.when(keeps)(lambda: o_own_line(0))
+    middle = jnp.logical_and(has_up, has_down)
+    last = jnp.logical_not(middle)
+    near = range(1, levels - 1)
+    lower, upper = z < half_levels, z >= half_levels
+
     for load in loads[4:]:
         load.wait()
     vg_side(0)
-    for d in range(1, levels - 1):
+    for d in near:
         vg_line(0, d)
         if d == 1:
-            x_peer(y).wait_recv()
+            x_peer(0).wait_recv()
             normalise_first(y)
+            o_swapped(0)
+            pl.when(last)(lambda: o_own_line(0, has_up, has_down))
             x_side().wait_recv()
-            x_peer(1 - y).start()
-    @pl.when(swaps)
-    def _():
-        o_swap(0).wait_recv()
-        o_own_line(0)
-
+            x_peer(1).start()
+    pl.when(middle)(lambda: o_own_line(0, lower, upper))
     o_own_here(0)
     vg_line(0, levels - 1)
-    x_peer(1 - y).wait_recv()
+    x_peer(1).wait_recv()
     normalise_first(1 - y)
     vg_other(0)
+    pl.when(middle)(lambda: o_own_line(0, upper, lower))
     glu(0)
-    middle = jnp.logical_and(has_up, has_down)
-    last = jnp.logical_not(middle)
 
     def o_near(l, *distances):
         for d in distances:
             o_line(l, d)
 
-    pl.when(middle)(lambda: o_near(0, *range(1, levels - 1)))
+    pl.when(middle)(lambda: o_near(0, *near))
     vg_own(1)
     vg_side(1)
     conv(0, y)
@@ -510,13 +560,8 @@
     take_glu(0)
     conv(0, 1 - y)
     o_across(0, step(0))
-    pl.when(last)(lambda: o_near(0, *range(2, levels - 1)))
-
-    def between(l):
-        o_line(l, levels - 1)
-        o_across(l, step(1))
-
-    activate(0, lambda: between(0))
+    pl.when(last)(lambda: o_near(0, *near[1:], levels - 1))
+    activate(0, lambda: o_across(0, step(1)))
     project_first(step(0))
     o_across(0, step(2))
     project_first(step(1))
@@ -526,46 +571,52 @@
             o_across(0, step(i))
         project_first(step(i))
     pl.when(last)(lambda: vg_line(1, 1))
-    for i in range(levels):
+    for i in range(0, levels, 2):
+        x1_peer(0, step(i)).wait_recv()
+        x1_peer(0, step(i + 1)).wait_recv()
+        x1_diagonal(step(i + 1)).start()
         x1_side(step(i)).wait_recv()
-        if i % 2 == 0:
-            x1_peer(1 - y, step(i)).start()
-        x1_peer(y, step(i)).wait_recv()
-        if i % 2 == 1:
-            x1_diagonal(step(i)).start()
-    for d in range(2, levels - 1):
+        x1_peer(1, step(i)).start()
+        x1_side(step(i + 1)).wait_recv()
+    for d in near[1:]:
         vg_line(1, d)
     normalise_next(y)
-
-    @pl.when(swaps)
-    def _():
-        o_swap(1).wait_recv()
-
-    o_own_line(1)
+    o_swapped(1)
+    pl.when(last)(lambda: o_own_line(1, has_up, has_down))
+    pl.when(middle)(lambda: o_own_line(1, lower, upper))
     o_own_here(1)
     for i in range(levels):
         if i % 2 == 0:
-            x1_peer(1 - y, step(i)).wait_recv()
+            x1_peer(1, step(i)).wait_recv()
         else:
             x1_diagonal(step(i)).wait_recv()
     normalise_next(1 - y)
     vg_line(1, levels - 1)
+    early = jnp.logical_and(last, core == 1)
+    late = jnp.logical_and(last, core == 0)
+    pl.when(early)(lambda: o_near(1, 1))
     vg_other(1)
     glu(1)
-    pl.when(middle)(lambda: o_near(1, *range(1, levels - 1)))
+
+    @pl.when(middle)
+    def _():
+        o_own_line(1, upper, lower)
+        o_near(1, *near)
+
     conv(1, y)
-    pl.when(last)(lambda: o_near(1, 1))
+    pl.when(early)(lambda: o_near(1, *near[1:]))
+    pl.when(late)(lambda: o_near(1, 1))
     take_glu(1)
     conv(1, 1 - y)
     o_across(1, step(0))
-    pl.when(last)(lambda: o_near(1, *range(2, levels - 1)))
-    activate(1, lambda: between(1))
-    squares = jnp.zeros((rows, 1), jnp.float32)
-    for i in range(levels):
-        if i > 0 and i < levels - 1:
-            o_across(1, step(i + 1))
-        o_other(1, step(i))
+    pl.when(early)(lambda: o_near(1, levels - 1))
+    pl.when(late)(lambda: o_near(1, *near[1:], levels - 1))
+    activate(1, lambda: o_across(1, step(1)))
+    squares = project_last(step(0))
+    for i in range(1, levels - 1):
+        o_across(1, step(i + 1)) if i + 1 < levels - 1 else None
         squares = squares + project_last(step(i))
+    squares = squares + project_end(step(levels - 1))
     st[...] = jnp.broadcast_to(squares, (rows, 128)).T[0:8]
     stat_copy().start()
 
@@ -574,32 +625,27 @@
         def _():
             for sem, count in ((upsem, zz + 1 if zz < levels - 1 else 0), (downsem, levels - zz if zz > 0 else 0)):
                 if count:
-                    block = vg.at[0 : 3 * LAYERS * count]
-                    pltpu.make_async_copy(block, block, sem).wait()
-    for sem, count in ((coresem, 2 * n), (sidesem, LAYERS + LAYERS * levels + 2 + levels // 2 + levels // 4 + LAYERS // 2)):
-        block = vg.at[0:count]
-        pltpu.make_async_copy(block, block, sem).wait()
-    for l in range(LAYERS):
-        pl.when(swaps)(lambda: o_swap(l).wait_send())
-        for yy in range(2):
-            pl.when(follows(yy))(lambda: halo(l, yy).wait_send())
+                    landed(vg.at[0 : 3 * LAYERS * count], sem)
+    landed(vg.at[0 : 2 * n], coresem)
+    landed(vg.at[0 : LAYERS + LAYERS * levels + 2 + levels // 2 + levels // 4 + LAYERS // 2], sidesem)
+    pl.when(swaps)(lambda: landed(osw, swsem.at[0]))
+    for yy in range(2):
+        pl.when(follows(yy))(lambda: landed(gl.at[0], hssem.at[yy]))
 
     stat_copy().wait_recv()
+    landed(x2r.at[0:half_levels], x2sem)
     both = st[...] + rst[...]
     total = jnp.concatenate([both] * (128 // 8), axis=0).T[:, 0:1]
     scale = lax.rsqrt(total / D + EPS)
     for i in range(half_levels):
         zz = tp * half_levels + i
-        x2_copy(zz).wait_recv()
-        for source, parity in ((x2, tp), (x2r, peer)):
-            for part in range(2):
+        for part in range(2):
+            for source, parity in ((x2, tp), (x2r, peer)):
                 at = ((i * 2 + part) * 2 + parity) * width
                 gain = fg_ref[0:1, pl.ds(pl.multiple_of(tp * cols + at, 128), width)]
-                value = source[zz, :, part * width : (part + 1) * width].astype(jnp.float32)
+                value = source[zz, part].astype(jnp.float32)
                 out_ref[:, pl.ds(pl.multiple_of(at, 128), width)] = (value * scale * gain).astype(jnp.bfloat16)
-    count = 4 + levels // 2 + levels // 4 + LAYERS + levels // 4
-    block = vg.at[0:count]
-    pltpu.make_async_copy(block, block, xsem).wait()
+    landed(vg.at[0 : 4 + levels // 2 + levels // 4 + LAYERS + levels // 4], xsem)
     stat_copy().wait_send()
 
 
@@ -618,17 +664,17 @@
         in_specs=[pl.BlockSpec(memory_space=pl.ANY)] * 9,
         out_specs=pl.BlockSpec(memory_space=pltpu.VMEM),
         scratch_shapes=[pltpu.VMEM(array.shape, array.dtype) for array in arrays[1:]] + [
-            dma((len(arrays),)),
+            dma((len(arrays) - 1,)),
             pltpu.VMEM((LAYERS * n, depth, ch), bf16),
             pltpu.VMEM((LAYERS, depth, ch), bf16),
             pltpu.VMEM((LAYERS, n, ch, width), bf16),
             pltpu.VMEM((LAYERS, ch, width), bf16),
             pltpu.VMEM((2, 2, rows, cols), bf16),
-            pltpu.VMEM((2, 2, levels, rows, 2 * width), bf16),
-            pltpu.VMEM((levels, rows, 2 * width), bf16),
-            pltpu.VMEM((levels, rows, 2 * width), bf16),
+            pltpu.VMEM((2, 2, levels, 2, rows, width), bf16),
+            pltpu.VMEM((levels, 2, rows, width), bf16),
+            pltpu.VMEM((levels, 2, rows, width), bf16),
             pltpu.VMEM((2, rows, 2 * cols), bf16),
-            pltpu.VMEM((LAYERS, 2, rows, ch // 2), f32),
+            pltpu.VMEM((LAYERS, 2, HALO, ch // 2), f32),
             pltpu.VMEM((LAYERS, rows, ch // 2), bf16),
             pltpu.VMEM((LAYERS, rows, ch // 2), bf16),
             pltpu.VMEM((LAYERS, 2, HALO + rows, ch // 2), f32),
@@ -639,16 +685,19 @@
             pltpu.VMEM((8, rows), f32),
             pltpu.VMEM((8, rows), f32),
             dma, dma, dma, dma, dma,
+            dma((LAYERS + 1,)),
+            dma((LAYERS, n // 2)),
+            dma((LAYERS,)),
+            dma((n // 2 + n,)),
+            dma((levels + n // 2,)),
+            dma((1 + LAYERS,)),
+            dma((3,)),
+            dma((3, levels)),
+            dma,
+            dma((LAYERS,)),
+            dma((LAYERS,)),
+            dma((2,)),
             dma((LAYERS, 2)),
-            dma((LAYERS, n)),
-            dma((LAYERS, n, 2)),
-            dma((LAYERS, 2)),
-            dma((2, 2)),
-            dma((2, 2, levels)),
-            dma((levels // 2,)),
-            dma((LAYERS, 2, 2)),
-            dma((LAYERS,)),
-            dma((LAYERS, 2, 2)),
             dma((2,)),
         ],
         compiler_params=pltpu.CompilerParams(collective_id=0, has_side_effects=True),

time: 71.8 us -> 69.2 us (0.964)
  Pallas kernels: 70.9 us -> 68.3 us
    pallas_call x1, Pallas kernels: 70.9 us -> 68.3 us  [fused(): pl.pallas_call(functools.partial(fused_kernel, n), out_shape=pltpu.VMEM((...]
where the time goes in v3:
time: 69.2 us; the launch traced here: 69 us
  Pallas kernels  68.3 us (99%)
  local copies, waits for them, and re-layouts  0.71 us (1%)
    pallas_call x1, Pallas kernels, fused(): pl.pallas_call(functools.partial(fused_kernel, n), out_shape=pltpu.VMEM((...  68.3 us

profile of v3, /device:TPU:0, one launch (start us, length us, event | category | flops | bytes accessed | tf_op | source)
XLA Modules:
  0.0 69.0 jit_solution(12095276674913678341)
XLA Ops:
  0.0 68.3 %shard_map.91 = bf16[128,1024]{1,0:T(8,128)(2,1)S(1)} custom-call(bf16[128,1024]{1,0:T(8,128)(2,1)} %x_in.1, f32[2,2048]{1,0:T(2,128)} %ng_in.1, bf16[256,512]{1,0:T(8,128)(2,1)} %v_in.1, bf16[256,512]{1,0:T(8,128)(2,1)} %g_in.1, f32[31,2,1024]{2,1,0:T(2,128)} %bitcast.2, f32[2,1024]{1,0:T(2,128)} %lng_in.1, f32[2,1024]{1,0:T(2,128)} %lnb_in.1, ...), custom_call_target="tpu_custom_call" | custom-call | tf_op jit(solution)/shard_map/pallas_call | solution.py:661
  68.3 0.7 %copy.11 = bf16[128,1024]{1,0:T(8,128)(2,1)} copy(bf16[128,1024]{1,0:T(8,128)(2,1)S(1)} %shard_map.91) | data formatting | bytes 524288

commit v4 on v3

--- a/solution.py
+++ b/solution.py
@@ -121,6 +121,10 @@
     width = ob.shape[3]
     has_up, has_down = z < levels - 1, z > 0
     swaps = tp + core == 1
+    middle = jnp.logical_and(has_up, has_down)
+    last = jnp.logical_not(middle)
+    near = range(1, levels - 1)
+    lower, upper = z < half_levels, z >= half_levels
     side, twin = sp + 2 - 4 * y, sp + 1 - 2 * core
 
     def index(zz, yy, cc):
@@ -270,7 +274,11 @@
             for half in halves(l):
                 o_take(l, src, half)
                 onward(l, src, half)
-                o_here(l, src, half)
+                if l == LAYERS - 1 and d == 1:
+                    pl.when(middle)(lambda: o_copy(l, src, half, sidesem, side).start())
+                    o_core(l, src, half)
+                else:
+                    o_here(l, src, half)
 
         pl.when(z - d >= 0)(lambda: one(z - d, o_up))
         pl.when(z + d < levels)(lambda: one(z + d, o_down))
@@ -280,6 +288,12 @@
         for half in halves(l):
             o_take(l, src, half)
             o_core(l, src, half)
+
+    def o_across_end(l):
+        src = index(z, 1 - y, core)
+        for half in halves(l):
+            pl.when(z == 1)(lambda: o_copy(l, src, half, downsem, sp - 4).start())
+            pl.when(z == levels - 2)(lambda: o_copy(l, src, half, upsem, sp + 4).start())
 
     def o_other_both(zz):
         landed(ob.at[0, 0:2], ocsem.at[zz])
@@ -480,20 +494,14 @@
         added = branch(1, zz)
         return put_last(zz, 0, added[:, :width]) + put_last(zz, 1, added[:, width:])
 
-    def project_end(zz):
-        total = None
-        for part in (y, 1 - y):
-            if total is not None:
-                o_across(1, zz)
-            o_other(zz, part)
-            added = None
-            for cc in range(2):
-                one = jnp.dot(act[cc], ob[1, index(zz, part, cc)], preferred_element_type=jnp.float32)
-                one = one.astype(jnp.bfloat16).astype(jnp.float32)
-                added = one if added is None else added + one
-            one = put_last(zz, part, added)
-            total = one if total is None else total + one
-        return total
+    def project_part(zz, part):
+        o_other(zz, part)
+        added = None
+        for cc in range(2):
+            one = jnp.dot(act[cc], ob[1, index(zz, part, cc)], preferred_element_type=jnp.float32)
+            one = one.astype(jnp.bfloat16).astype(jnp.float32)
+            added = one if added is None else added + one
+        return put_last(zz, part, added)
 
     def stat_copy():
         return remote(st, rst, tsem.at[0], tsem.at[1], sp, peer)
@@ -522,11 +530,6 @@
     loads[3].wait()
     for l in range(LAYERS):
         pick_columns(l)
-    middle = jnp.logical_and(has_up, has_down)
-    last = jnp.logical_not(middle)
-    near = range(1, levels - 1)
-    lower, upper = z < half_levels, z >= half_levels
-
     for load in loads[4:]:
         load.wait()
     vg_side(0)
@@ -602,21 +605,38 @@
     def _():
         o_own_line(1, upper, lower)
         o_near(1, *near)
+        o_across(1, z)
+        o_across_end(1)
 
     conv(1, y)
     pl.when(early)(lambda: o_near(1, *near[1:]))
     pl.when(late)(lambda: o_near(1, 1))
     take_glu(1)
     conv(1, 1 - y)
-    o_across(1, step(0))
+    pl.when(last)(lambda: o_across(1, z))
     pl.when(early)(lambda: o_near(1, levels - 1))
     pl.when(late)(lambda: o_near(1, *near[1:], levels - 1))
-    activate(1, lambda: o_across(1, step(1)))
-    squares = project_last(step(0))
-    for i in range(1, levels - 1):
-        o_across(1, step(i + 1)) if i + 1 < levels - 1 else None
-        squares = squares + project_last(step(i))
-    squares = squares + project_end(step(levels - 1))
+    at_end = last.astype(jnp.int32)
+
+    def order(i):
+        if i == 0:
+            return step(0)
+        return step(i + at_end if i < levels - 1 else levels - 1 - at_end * (levels - 2))
+
+    activate(1, lambda: None)
+    squares = project_last(order(0))
+
+    @pl.when(core == 1)
+    def _():
+        for i in range(1, levels):
+            o_across(1, order(i))
+
+    squares = squares + project_part(order(levels - 1), y)
+    for i in near:
+        pl.when(core == 0)(lambda: o_across(1, order(i)))
+        squares = squares + project_last(order(i))
+    pl.when(core == 0)(lambda: o_across(1, order(levels - 1)))
+    squares = squares + project_part(order(levels - 1), 1 - y)
     st[...] = jnp.broadcast_to(squares, (rows, 128)).T[0:8]
     stat_copy().start()
 
@@ -624,10 +644,13 @@
         @pl.when(z == zz)
         def _():
             for sem, count in ((upsem, zz + 1 if zz < levels - 1 else 0), (downsem, levels - zz if zz > 0 else 0)):
+                extra = (zz == levels - 2) if sem is upsem else (zz == 1)
                 if count:
-                    landed(vg.at[0 : 3 * LAYERS * count], sem)
+                    landed(vg.at[0 : 3 * LAYERS * count + extra], sem)
     landed(vg.at[0 : 2 * n], coresem)
-    landed(vg.at[0 : LAYERS + LAYERS * levels + 2 + levels // 2 + levels // 4 + LAYERS // 2], sidesem)
+    count = LAYERS + LAYERS * levels + 2 + levels // 2 + levels // 4 + LAYERS // 2
+    pl.when(middle)(lambda: landed(vg.at[0:count], sidesem))
+    pl.when(last)(lambda: landed(vg.at[0 : count - 1], sidesem))
     pl.when(swaps)(lambda: landed(osw, swsem.at[0]))
     for yy in range(2):
         pl.when(follows(yy))(lambda: landed(gl.at[0], hssem.at[yy]))
@@ -710,7 +733,7 @@
 
     def step(*args):
         stream, out_weight = args[0], args[7]
-        fits = (n_tp == 2 and n % 8 == 0 and stream.shape[0] == 128 and out_weight.shape[1] == 128 * LAYERS
+        fits = (n_tp == 2 and n % 8 == 0 and n > 8 and stream.shape[0] == 128 and out_weight.shape[1] == 128 * LAYERS
                 and args[2].shape == (128 * LAYERS, 512))
         return fused(n, *args) if fits else local(*args)
 

time: 69.2 us -> 68.1 us (0.984)
  Pallas kernels: 68.3 us -> 67.3 us
    pallas_call x1, Pallas kernels: 68.3 us -> 67.3 us  [fused(): pl.pallas_call(functools.partial(fused_kernel, n), out_shape=pltpu.VMEM((...]
where the time goes in v4:
time: 68.1 us; the launch traced here: 68 us
  Pallas kernels  67.3 us (99%)
  local copies, waits for them, and re-layouts  0.71 us (1%)
    pallas_call x1, Pallas kernels, fused(): pl.pallas_call(functools.partial(fused_kernel, n), out_shape=pltpu.VMEM((...  67.3 us

profile of v4, /device:TPU:0, one launch (start us, length us, event | category | flops | bytes accessed | tf_op | source)
XLA Modules:
  0.0 68.0 jit_solution(7370258904932059907)
XLA Ops:
  0.0 67.3 %shard_map.91 = bf16[128,1024]{1,0:T(8,128)(2,1)S(1)} custom-call(bf16[128,1024]{1,0:T(8,128)(2,1)} %x_in.1, f32[2,2048]{1,0:T(2,128)} %ng_in.1, bf16[256,512]{1,0:T(8,128)(2,1)} %v_in.1, bf16[256,512]{1,0:T(8,128)(2,1)} %g_in.1, f32[31,2,1024]{2,1,0:T(2,128)} %bitcast.2, f32[2,1024]{1,0:T(2,128)} %lng_in.1, f32[2,1024]{1,0:T(2,128)} %lnb_in.1, ...), custom_call_target="tpu_custom_call" | custom-call | tf_op jit(solution)/shard_map/pallas_call | solution.py:684
  67.3 0.7 %copy.11 = bf16[128,1024]{1,0:T(8,128)(2,1)} copy(bf16[128,1024]{1,0:T(8,128)(2,1)S(1)} %shard_map.91) | data formatting | bytes 524288

commit v5 on v4

--- a/solution.py
+++ b/solution.py
@@ -268,7 +268,7 @@
         for half in halves(l):
             o_here(l, sp, half)
 
-    def o_line(l, d):
+    def o_line(l, d, below=True, above=True):
         def one(zz, onward):
             src = index(zz, y, core)
             for half in halves(l):
@@ -280,8 +280,8 @@
                 else:
                     o_here(l, src, half)
 
-        pl.when(z - d >= 0)(lambda: one(z - d, o_up))
-        pl.when(z + d < levels)(lambda: one(z + d, o_down))
+        pl.when(jnp.logical_and(z - d >= 0, below))(lambda: one(z - d, o_up))
+        pl.when(jnp.logical_and(z + d < levels, above))(lambda: one(z + d, o_down))
 
     def o_across(l, zz):
         src = index(zz, 1 - y, core)
@@ -558,6 +558,8 @@
     pl.when(middle)(lambda: o_near(0, *near))
     vg_own(1)
     vg_side(1)
+    o_swapped(1)
+    pl.when(last)(lambda: o_own_line(1, has_up, has_down))
     conv(0, y)
     pl.when(last)(lambda: o_near(0, 1))
     take_glu(0)
@@ -584,10 +586,14 @@
     for d in near[1:]:
         vg_line(1, d)
     normalise_next(y)
-    o_swapped(1)
-    pl.when(last)(lambda: o_own_line(1, has_up, has_down))
     pl.when(middle)(lambda: o_own_line(1, lower, upper))
     o_own_here(1)
+
+    @pl.when(middle)
+    def _():
+        for d in near:
+            o_line(1, d, lower, upper)
+
     for i in range(levels):
         if i % 2 == 0:
             x1_peer(1, step(i)).wait_recv()
@@ -597,25 +603,26 @@
     vg_line(1, levels - 1)
     early = jnp.logical_and(last, core == 1)
     late = jnp.logical_and(last, core == 0)
-    pl.when(early)(lambda: o_near(1, 1))
+    pl.when(early)(lambda: o_near(1, 2))
     vg_other(1)
     glu(1)
 
     @pl.when(middle)
     def _():
+        for d in near:
+            o_line(1, d, upper, lower)
         o_own_line(1, upper, lower)
-        o_near(1, *near)
         o_across(1, z)
         o_across_end(1)
 
     conv(1, y)
-    pl.when(early)(lambda: o_near(1, *near[1:]))
-    pl.when(late)(lambda: o_near(1, 1))
+    pl.when(early)(lambda: o_near(1, *range(3, levels)))
+    pl.when(late)(lambda: o_near(1, 2))
     take_glu(1)
     conv(1, 1 - y)
     pl.when(last)(lambda: o_across(1, z))
-    pl.when(early)(lambda: o_near(1, levels - 1))
-    pl.when(late)(lambda: o_near(1, *near[1:], levels - 1))
+    pl.when(early)(lambda: o_near(1, 1))
+    pl.when(late)(lambda: o_near(1, *range(3, levels), 1))
     at_end = last.astype(jnp.int32)
 
     def order(i):
@@ -644,9 +651,10 @@
         @pl.when(z == zz)
         def _():
             for sem, count in ((upsem, zz + 1 if zz < levels - 1 else 0), (downsem, levels - zz if zz > 0 else 0)):
+                count *= 3 * LAYERS
                 extra = (zz == levels - 2) if sem is upsem else (zz == 1)
                 if count:
-                    landed(vg.at[0 : 3 * LAYERS * count + extra], sem)
+                    landed(vg.at[0 : count + extra], sem)
     landed(vg.at[0 : 2 * n], coresem)
     count = LAYERS + LAYERS * levels + 2 + levels // 2 + levels // 4 + LAYERS // 2
     pl.when(middle)(lambda: landed(vg.at[0:count], sidesem))

time: 68.1 us -> 66.4 us (0.975)
  Pallas kernels: 67.3 us -> 65.6 us
    pallas_call x1, Pallas kernels: 67.3 us -> 65.6 us  [fused(): pl.pallas_call(functools.partial(fused_kernel, n), out_shape=pltpu.VMEM((...]
where the time goes in v5:
time: 66.4 us; the launch traced here: 66.3 us
  Pallas kernels  65.6 us (99%)
  local copies, waits for them, and re-layouts  0.71 us (1%)
    pallas_call x1, Pallas kernels, fused(): pl.pallas_call(functools.partial(fused_kernel, n), out_shape=pltpu.VMEM((...  65.6 us

profile of v5, /device:TPU:0, one launch (start us, length us, event | category | flops | bytes accessed | tf_op | source)
XLA Modules:
  0.0 66.3 jit_solution(10576661025488019318)
XLA Ops:
  0.0 65.6 %shard_map.91 = bf16[128,1024]{1,0:T(8,128)(2,1)S(1)} custom-call(bf16[128,1024]{1,0:T(8,128)(2,1)} %x_in.1, f32[2,2048]{1,0:T(2,128)} %ng_in.1, bf16[256,512]{1,0:T(8,128)(2,1)} %v_in.1, bf16[256,512]{1,0:T(8,128)(2,1)} %g_in.1, f32[31,2,1024]{2,1,0:T(2,128)} %bitcast.2, f32[2,1024]{1,0:T(2,128)} %lng_in.1, f32[2,1024]{1,0:T(2,128)} %lnb_in.1, ...), custom_call_target="tpu_custom_call" | custom-call | tf_op jit(solution)/shard_map/pallas_call | solution.py:692
  65.6 0.7 %copy.11 = bf16[128,1024]{1,0:T(8,128)(2,1)} copy(bf16[128,1024]{1,0:T(8,128)(2,1)S(1)} %shard_map.91) | data formatting | bytes 524288

commit v6 on v5

--- a/solution.py
+++ b/solution.py
@@ -373,12 +373,12 @@
     def halo(l, yy):
         return remote(
             gl.at[l, yy], ext.at[l, y, pl.ds(0, HALO)],
-            hssem.at[yy], hsem.at[l, y], index(z, yy, core) + 1, tp)
+            hssem, hsem.at[l, y], index(z, yy, core) + 1, tp)
 
     def halo_wait(l, q):
         remote(
             gl.at[l, 0], ext.at[l, q, pl.ds(0, HALO)],
-            hssem.at[0], hsem.at[l, q], side, tp).wait_recv()
+            hssem, hsem.at[l, q], side, tp).wait_recv()
 
     def glu(l):
         weights = vg[l * n : (l + 1) * n].reshape(n * depth, 2 * quarter)
@@ -456,19 +456,19 @@
         return total
 
     def x1_side(zz):
-        return same(x1.at[y, tp, zz], sidesem, x1sem.at[0, zz], side)
-
-    def x1_peer(far, zz):
+        return same(x1.at[y, tp, zz], sidesem, x1sem.at[zz], side)
+
+    def x1_peer(far, zz, i):
         block = x1.at[1 - y if far else y, tp, zz]
-        return remote(block, block, xsem, x1sem.at[1 + far, zz], sp, peer)
+        return remote(block, block, xsem, x1sem.at[levels + (half_levels if far else i // 2)], sp, peer)
 
     def x1_diagonal(zz):
-        return same(x1.at[y, peer, zz], sidesem, x1sem.at[2, zz], side)
+        return same(x1.at[y, peer, zz], sidesem, x1sem.at[levels + half_levels + 1], side)
 
     def step(i):
         return (z + levels + (1 - 2 * (z // half_levels)) * i) % levels
 
-    def project_first(zz):
+    def project_first(zz, i):
         o_other_both(zz)
         added = branch(0, zz)
         for part in range(2):
@@ -477,7 +477,7 @@
             x1[y, tp, zz, part] = (
                 here + added[:, part * width : (part + 1) * width]).astype(jnp.bfloat16)
         x1_side(zz).start()
-        x1_peer(0, zz).start()
+        x1_peer(0, zz, i).start()
 
     def x2_copy(zz, part):
         return remote(x2.at[zz, part], x2r.at[zz, part], xsem, x2sem, sp, peer)
@@ -494,14 +494,16 @@
         added = branch(1, zz)
         return put_last(zz, 0, added[:, :width]) + put_last(zz, 1, added[:, width:])
 
-    def project_part(zz, part):
-        o_other(zz, part)
+    def project_pair(planes, part):
+        for zz in planes:
+            o_other(zz, part)
         added = None
         for cc in range(2):
-            one = jnp.dot(act[cc], ob[1, index(zz, part, cc)], preferred_element_type=jnp.float32)
+            weights = jnp.concatenate([ob[1, index(zz, part, cc)] for zz in planes], axis=1)
+            one = jnp.dot(act[cc], weights, preferred_element_type=jnp.float32)
             one = one.astype(jnp.bfloat16).astype(jnp.float32)
             added = one if added is None else added + one
-        return put_last(zz, part, added)
+        return sum(put_last(zz, part, added[:, k * width : (k + 1) * width]) for k, zz in enumerate(planes))
 
     def stat_copy():
         return remote(st, rst, tsem.at[0], tsem.at[1], sp, peer)
@@ -567,21 +569,20 @@
     o_across(0, step(0))
     pl.when(last)(lambda: o_near(0, *near[1:], levels - 1))
     activate(0, lambda: o_across(0, step(1)))
-    project_first(step(0))
+    project_first(step(0), 0)
     o_across(0, step(2))
-    project_first(step(1))
+    project_first(step(1), 1)
     pl.when(middle)(lambda: vg_line(1, 1))
     for i in range(2, levels):
         if i > 2:
             o_across(0, step(i))
-        project_first(step(i))
+        project_first(step(i), i)
     pl.when(last)(lambda: vg_line(1, 1))
     for i in range(0, levels, 2):
-        x1_peer(0, step(i)).wait_recv()
-        x1_peer(0, step(i + 1)).wait_recv()
+        landed(x1.at[0, 0, 0:2], x1sem.at[levels + i // 2])
         x1_diagonal(step(i + 1)).start()
         x1_side(step(i)).wait_recv()
-        x1_peer(1, step(i)).start()
+        x1_peer(1, step(i), i).start()
         x1_side(step(i + 1)).wait_recv()
     for d in near[1:]:
         vg_line(1, d)
@@ -594,11 +595,8 @@
         for d in near:
             o_line(1, d, lower, upper)
 
-    for i in range(levels):
-        if i % 2 == 0:
-            x1_peer(1, step(i)).wait_recv()
-        else:
-            x1_diagonal(step(i)).wait_recv()
+    for i in range(2):
+        landed(x1.at[0, 0, 0:half_levels], x1sem.at[levels + half_levels + i])
     normalise_next(1 - y)
     vg_line(1, levels - 1)
     early = jnp.logical_and(last, core == 1)
@@ -622,7 +620,7 @@
     conv(1, 1 - y)
     pl.when(last)(lambda: o_across(1, z))
     pl.when(early)(lambda: o_near(1, 1))
-    pl.when(late)(lambda: o_near(1, *range(3, levels), 1))
+    pl.when(late)(lambda: o_near(1, *range(3, levels)))
     at_end = last.astype(jnp.int32)
 
     def order(i):
@@ -630,20 +628,28 @@
             return step(0)
         return step(i + at_end if i < levels - 1 else levels - 1 - at_end * (levels - 2))
 
+    pl.when(late)(lambda: o_across(1, order(1)))
     activate(1, lambda: None)
     squares = project_last(order(0))
+    pl.when(late)(lambda: o_near(1, 1))
 
     @pl.when(core == 1)
     def _():
         for i in range(1, levels):
             o_across(1, order(i))
 
-    squares = squares + project_part(order(levels - 1), y)
-    for i in near:
-        pl.when(core == 0)(lambda: o_across(1, order(i)))
+    for i in near[:-1]:
+        pl.when(jnp.logical_and(middle, core == 0) if i == 1 else core == 0)(lambda: o_across(1, order(i)))
         squares = squares + project_last(order(i))
-    pl.when(core == 0)(lambda: o_across(1, order(levels - 1)))
-    squares = squares + project_part(order(levels - 1), 1 - y)
+    pair = (order(levels - 2), order(levels - 1))
+    squares = squares + project_pair(pair, y)
+
+    @pl.when(core == 0)
+    def _():
+        for zz in pair:
+            o_across(1, zz)
+
+    squares = squares + project_pair(pair, 1 - y)
     st[...] = jnp.broadcast_to(squares, (rows, 128)).T[0:8]
     stat_copy().start()
 
@@ -660,8 +666,8 @@
     pl.when(middle)(lambda: landed(vg.at[0:count], sidesem))
     pl.when(last)(lambda: landed(vg.at[0 : count - 1], sidesem))
     pl.when(swaps)(lambda: landed(osw, swsem.at[0]))
-    for yy in range(2):
-        pl.when(follows(yy))(lambda: landed(gl.at[0], hssem.at[yy]))
+    pl.when(follows(1))(lambda: landed(gl, hssem))
+    pl.when(jnp.logical_not(follows(1)))(lambda: landed(gl.at[0], hssem))
 
     stat_copy().wait_recv()
     landed(x2r.at[0:half_levels], x2sem)
@@ -723,11 +729,11 @@
             dma((levels + n // 2,)),
             dma((1 + LAYERS,)),
             dma((3,)),
-            dma((3, levels)),
+            dma((levels + levels // 2 + 2,)),
             dma,
             dma((LAYERS,)),
             dma((LAYERS,)),
-            dma((2,)),
+            dma,
             dma((LAYERS, 2)),
             dma((2,)),
         ],

time: 66.4 us -> 66.5 us (level)
  no operation moved by 1% of the time
where the time goes in v6:
time: 66.5 us; the launch traced here: 66.3 us
  Pallas kernels  65.6 us (99%)
  local copies, waits for them, and re-layouts  0.71 us (1%)
    pallas_call x1, Pallas kernels, fused(): pl.pallas_call(functools.partial(fused_kernel, n), out_shape=pltpu.VMEM((...  65.6 us

profile of v6, /device:TPU:0, one launch (start us, length us, event | category | flops | bytes accessed | tf_op | source)
XLA Modules:
  0.0 66.3 jit_solution(18422846340947569363)
XLA Ops:
  0.0 65.6 %shard_map.91 = bf16[128,1024]{1,0:T(8,128)(2,1)S(1)} custom-call(bf16[128,1024]{1,0:T(8,128)(2,1)} %x_in.1, f32[2,2048]{1,0:T(2,128)} %ng_in.1, bf16[256,512]{1,0:T(8,128)(2,1)} %v_in.1, bf16[256,512]{1,0:T(8,128)(2,1)} %g_in.1, f32[31,2,1024]{2,1,0:T(2,128)} %bitcast.2, f32[2,1024]{1,0:T(2,128)} %lng_in.1, f32[2,1024]{1,0:T(2,128)} %lnb_in.1, ...), custom_call_target="tpu_custom_call" | custom-call | tf_op jit(solution)/shard_map/pallas_call | solution.py:698
  65.6 0.7 %copy.11 = bf16[128,1024]{1,0:T(8,128)(2,1)} copy(bf16[128,1024]{1,0:T(8,128)(2,1)S(1)} %shard_map.91) | data formatting | bytes 524288
